TPU v7x, 32 devices: a whole 2x2x4 slice. The times are simulated.
32 devices in a mesh: ep: 4 (over y, x), tp: 8 (over z, core).
Axes of the slice: x: 2, y: 2, z: 4, core: 2. Of those that a mesh axis runs over, the one named last changes fastest.
Arguments:
- tokens: bfloat16 [512, 2048], P('ep'), may hold values from -32 to 32
- routes: int32 [512, 2], P('ep'), may hold values from 0 to 3, all different within a row; in each aligned block of 128 rows (0 to 127, 128 to 255, ...) at most 96 rows name the same one
- gates: float32 [512, 2], P('ep'), may hold values from 0.05 to 0.6
- cotangent: bfloat16 [512, 2048], P('ep'), may hold values from -6 to 6
- w_glu: bfloat16 [4, 2048, 1024], P('ep', None, 'tp'), may hold values from -0.125 to 0.125
- w_lin: bfloat16 [4, 2048, 1024], P('ep', None, 'tp'), may hold values from -0.125 to 0.125
- w_down: bfloat16 [4, 1024, 2048], P('ep', 'tp'), may hold values from -0.1875 to 0.1875
Outputs:
- d_tokens: bfloat16 [512, 2048], P('ep', 'tp')
- d_gates: float32 [512, 2], P('ep')
- glu_wgrad: float32 [4, 2048, 1024], P('ep', None, 'tp')
- lin_wgrad: float32 [4, 2048, 1024], P('ep', None, 'tp')
- down_wgrad: float32 [4, 1024, 2048], P('ep', 'tp')
- glu_norms: float32 [4, 2048], P('ep')
- lin_norms: float32 [4, 2048], P('ep')
- down_norms: float32 [4, 1024], P('ep', 'tp')
Inputs may be any that keep to these rules, and one draw needn't show every extreme that they name: `routes`: each row names 2 different experts. Among the 128 tokens of one aligned block no expert is named more than 96 times, and in every draw some expert is named exactly 96 times in some block.
All inputs are finite; a program needn't handle non-finite values.
Results may differ from a plain program's by a relative error of at most 0.024.
Values may be sent and summed in bfloat16 or wider, within the bound.
A program may use at most 64 MiB of HBM per device.

v0:
```python
import functools

import jax
import jax.numpy as jnp
from jax import lax
from jax.experimental import pallas as pl
from jax.experimental.pallas import tpu as pltpu
from jax.sharding import PartitionSpec as P

clamp_limit = 7.0
sigmoid_scale = 1.702
MESH = pl.DeviceIdType.MESH
LANES = 128
CORES = 2
f32 = jnp.float32
bf16 = jnp.bfloat16


def dot_nn(a, b):
    return lax.dot_general(a, b, (((1,), (0,)), ((), ())), preferred_element_type=f32)


def dot_nt(a, b):
    return lax.dot_general(a, b, (((1,), (1,)), ((), ())), preferred_element_type=f32)


def clamp_backward(glu_pre, lin_pre, back_proj, gate_col):
    glu_clip = jnp.minimum(glu_pre, clamp_limit)
    lin_clip = jnp.clip(lin_pre, -clamp_limit, clamp_limit)
    sig_val = jax.nn.sigmoid(sigmoid_scale * glu_clip)
    glu_act = glu_clip * sig_val
    hidden = glu_act * (lin_clip + 1.0)
    hid_grad = gate_col * back_proj
    act_slope = sig_val + sigmoid_scale * glu_clip * sig_val * (1.0 - sig_val)
    glu_grad = jnp.where(glu_pre < clamp_limit, hid_grad * (lin_clip + 1.0) * act_slope, 0.0)
    lin_grad = jnp.where(jnp.abs(lin_pre) < clamp_limit, hid_grad * glu_act, 0.0)
    return hidden, glu_grad.astype(bf16), lin_grad.astype(bf16)


def kernel(
    ep, tp, cap,
    tok_hbm, routes_hbm, gates_hbm, cot_hbm, wg_hbm, wl_hbm, wd_hbm,
    dtok_ref, dgate_ref, gw_v, lw_v, dw_v, gn_ref, ln_ref, dn_ref,
    tok_ref, routes_ref, gates_ref, cot_ref, wg_ref, wl_ref, wd_ref,
    pt_v, pk_v, snd_v, all_v, gsnd_v, grow_v, bf_v, tr_v,
    ps_v, pr_v, mine_v, xs_v, ret_v, zs_v, zr_v,
    gp_v, gsum_v, gback_v, ns_v, nr_v,
    d_s, d_r, h_s, h_r, g_s, g_r, y_s, y_r, p_s, p_r, x_s, x_r, z_s, z_r,
    a_s, a_r, b_s, b_r, n_s, n_r, l_s,
):
    me = lax.axis_index("ep")
    tpi = lax.axis_index("tp")
    nz = tp // CORES
    core = lax.rem(tpi, CORES)
    chip = lax.div(tpi, CORES)
    other = 1 - core
    partner = chip * CORES + other
    rows = tok_ref.shape[0]
    width = tok_ref.shape[1]
    hidden_units = wg_ref.shape[1]
    half = width // CORES
    own = width // tp
    odd = lax.rem(chip, 2)
    beside = (chip + 1 - 2 * odd) * CORES + core
    loads = []
    for i, (src, dst) in enumerate((
        (routes_hbm, routes_ref), (gates_hbm, gates_ref), (cot_hbm, cot_ref),
        (tok_hbm, tok_ref), (wg_hbm, wg_ref), (wl_hbm, wl_ref), (wd_hbm, wd_ref),
    )):
        cp = pltpu.make_async_copy(src, dst, l_s.at[i])
        cp.start()
        loads.append(cp)

    def ahead(r):
        return lax.rem(me + r, ep)

    def behind(r):
        return lax.rem(me + ep - r, ep)

    barrier = pltpu.get_barrier_semaphore()
    for r in range(1, ep):
        pl.semaphore_signal(barrier, inc=1, device_id={"ep": ahead(r)}, device_id_type=MESH)
    for q in range(1, tp):
        pl.semaphore_signal(
            barrier, inc=1, device_id={"tp": lax.rem(tpi + q, tp)}, device_id_type=MESH
        )

    def remote(src, dst, ss, rs, where):
        return pltpu.make_async_remote_copy(
            src_ref=src, dst_ref=dst, send_sem=ss, recv_sem=rs,
            device_id=where, device_id_type=MESH,
        )

    loads[0].wait()
    loads[1].wait()
    rel = routes_ref[...] - me
    rel = jnp.where(rel < 0, rel + ep, rel)
    erows = gp_v.shape[1]
    sub = lax.broadcasted_iota(jnp.int32, (erows, rows), 0)
    first, second = sub == rel[0:1, :], sub == rel[1:2, :]
    mask = jnp.where(first, 1.0, 0.0) + jnp.where(second, 1.0, 0.0)
    gate_of = jnp.where(first, gates_ref[0:1, :], 0.0) + jnp.where(second, gates_ref[1:2, :], 0.0)
    before = lax.broadcasted_iota(jnp.int32, (rows, rows), 0) < lax.broadcasted_iota(
        jnp.int32, (rows, rows), 1
    )
    rank = dot_nn(mask.astype(bf16), jnp.where(before, 1.0, 0.0).astype(bf16))
    place = jnp.where(mask > 0.5, rank, -1.0)
    slot_at = lax.broadcasted_iota(jnp.int32, (LANES, rows), 0).astype(f32)
    hits = [jnp.where(slot_at == place[r:r + 1, :], 1.0, 0.0) for r in range(ep)]
    picks = [hit[:cap, :].astype(bf16) for hit in hits]
    square = lax.broadcasted_iota(jnp.int32, (LANES, LANES), 0) == lax.broadcasted_iota(
        jnp.int32, (LANES, LANES), 1
    )
    sends = []

    narrow = half // 8
    pieces = (
        (1, 0, half // 2, True),
        (0, 0, narrow, True),
        (0, 2 * narrow, half - 2 * narrow, False),
    )
    swapped = [i for i, piece in enumerate(pieces) if piece[3]]
    refs = (tok_ref, cot_ref)

    def window(i, whose):
        a, off, w, shared = pieces[i]
        if shared:
            off = off + whose * w
        return a, (pl.ds(pl.multiple_of(off, LANES), w) if shared else pl.ds(off, w))

    def area(buf, i, r, whose, which):
        a, cols = window(i, whose)
        return buf.at[a, which, pl.ds(r * cap, cap), cols]

    def dispatch(i, r):
        a, cols = window(i, odd)
        return remote(
            snd_v.at[a, r, :, cols], area(all_v, i, r, odd, core),
            d_s.at[i, r], d_r.at[i, r], {"ep": ahead(r)},
        )

    def swap(i, r, whose):
        at = area(all_v, i, r, whose, core)
        return remote(at, at, h_s.at[i, r], h_r.at[i, r], {"tp": beside})

    def relay(k, i, r, whose, which):
        at = area(all_v, i, r, whose, which)
        return remote(at, at, y_s.at[k, r], y_r.at[k, r], {"tp": partner})

    loads[2].wait()
    loads[3].wait()
    waited = False
    for i in range(len(pieces)):
        a, off, w, shared = pieces[i]
        start = core * half + off + (odd * w if shared else 0)
        src_cols = pl.ds(pl.multiple_of(start, LANES), w)
        for r in range(1, ep):
            snd_v[a, r, :, window(i, odd)[1]] = dot_nn(
                picks[r], refs[a][:, src_cols]
            ).astype(bf16)
            if not waited:
                pl.semaphore_wait(barrier, ep - 1 + tp - 1)
                waited = True
            cp = dispatch(i, r)
            cp.start()
            sends.append(cp)
    for r in range(ep):
        col = jnp.sum(hits[r] * gate_of[r:r + 1, :], axis=1, keepdims=True)
        row = jnp.sum(jnp.where(square, col, 0.0), axis=0, keepdims=True)
        if r == 0:
            grow_v[0] = jnp.broadcast_to(row, (8, LANES))
        else:
            gsnd_v[r] = jnp.broadcast_to(row, (8, LANES))
            cp = remote(gsnd_v.at[r], grow_v.at[r], g_s.at[r], g_r.at[r], {"ep": ahead(r)})
            cp.start()
            sends.append(cp)
    for a, ref in ((0, tok_ref), (1, cot_ref)):
        for h in range(CORES):
            all_v[a, h, 0:cap, :] = dot_nn(picks[0], ref[:, h * half:(h + 1) * half]).astype(bf16)
    for r in range(ep):
        pk_v[r] = hits[r].astype(bf16)
        pt_v[r] = hits[r].T.astype(bf16)

    eye = lax.broadcasted_iota(jnp.int32, (cap, LANES), 0) == lax.broadcasted_iota(
        jnp.int32, (cap, LANES), 1
    )

    gp_v[tpi] = jnp.zeros(gp_v.shape[1:], f32)

    def forward(r):
        rs = slice(r * cap, (r + 1) * cap)
        glu_pre = jnp.zeros((cap, hidden_units), f32)
        lin_pre = glu_pre
        back = glu_pre
        for h in range(CORES):
            hs = slice(h * half, (h + 1) * half)
            glu_pre = glu_pre + dot_nn(all_v[0, h, rs, :], wg_ref[hs, :])
            lin_pre = lin_pre + dot_nn(all_v[0, h, rs, :], wl_ref[hs, :])
            back = back + dot_nt(all_v[1, h, rs, :], wd_ref[:, hs])
        gate_col = jnp.sum(jnp.where(eye, grow_v[r, 0:1, :], 0.0), axis=1, keepdims=True)
        hidden, glu_bf, lin_bf = clamp_backward(glu_pre, lin_pre, back, gate_col)
        part = jnp.sum(back * hidden, axis=1, keepdims=True)
        gp_v[tpi, r:r + 1, :] = jnp.sum(jnp.where(eye, part, 0.0), axis=0, keepdims=True)
        bf_v[0, rs, :] = glu_bf
        bf_v[1, rs, :] = lin_bf
        bf_v[2, rs, :] = (gate_col * hidden).astype(bf16)

    count = len(pieces)
    for i in swapped:
        for r in range(1, ep):
            dispatch(i, r).wait_recv()
            for cp in (swap(i, r, odd), relay(i, i, r, odd, core)):
                cp.start()
                sends.append(cp)
    for cp in loads[4:]:
        cp.wait()
    forward(0)
    for r in range(1, ep):
        for n, i in enumerate(swapped):
            swap(i, r, 1 - odd).wait_recv()
            cp = relay(count + n, i, r, 1 - odd, core)
            cp.start()
            sends.append(cp)
        for i in range(count):
            if i not in swapped:
                dispatch(i, r).wait_recv()
                cp = relay(i, i, r, odd, core)
                cp.start()
                sends.append(cp)
    for r in range(1, ep):
        for i in range(count):
            relay(i, i, r, odd, other).wait_recv()
        for n, i in enumerate(swapped):
            relay(count + n, i, r, 1 - odd, other).wait_recv()
        remote(gsnd_v.at[r], grow_v.at[r], g_s.at[r], g_r.at[r], {"ep": ahead(r)}).wait_recv()
        forward(r)

    for q in range(1, tp):
        cp = remote(gp_v.at[tpi], gp_v.at[tpi], a_s.at[q], a_r.at[q], {"tp": lax.rem(tpi + q, tp)})
        cp.start()
        sends.append(cp)

    def input_cols(q, which):
        z = lax.rem(chip + q, nz)
        at = pl.ds(pl.multiple_of((z * CORES + which) * own, own), own)
        return dot_nt(bf_v[0], wg_ref[at, :]) + dot_nt(bf_v[1], wl_ref[at, :])

    order = list(range(1, nz)) + [0]
    for q in order:
        ps_v[q] = input_cols(q, other).astype(bf16)
        cp = remote(ps_v.at[q], pr_v.at[q], p_s.at[q], p_r.at[q], {"tp": partner})
        cp.start()
        sends.append(cp)
    for q in order:
        mine_v[q] = input_cols(q, core)
    for q in order:
        remote(ps_v.at[q], pr_v.at[q], p_s.at[q], p_r.at[q], {"tp": partner}).wait_recv()
        total = (mine_v[q] + pr_v[q].astype(f32)).astype(bf16)
        ret_v[q, 0:cap, :] = total[0:cap, :]
        for r in range(1, ep):
            rs = slice(r * cap, (r + 1) * cap)
            xs_v[q, rs, :] = total[rs, :]
        for r in range(1, ep):
            rs = pl.ds(r * cap, cap)
            cp = remote(
                xs_v.at[q, rs, :], ret_v.at[q, rs, :],
                x_s.at[q, r], x_r.at[q, r], {"ep": behind(r)},
            )
            cp.start()
            sends.append(cp)

    for i in range(3):
        tr_v[i] = bf_v[i].astype(f32).T.astype(bf16)
    step = min(512, half)
    for h in range(CORES):
        for c0 in range(0, half, step):
            cols = slice(h * half + c0, h * half + c0 + step)
            x = all_v[0, h, :, c0:c0 + step]
            for i, (w_v, at) in enumerate(((gw_v, 0), (lw_v, 1))):
                w = dot_nn(tr_v[i], x)
                ns_v[at:at + 1, cols] = jnp.sum(w * w, axis=0, keepdims=True)
                w_v[cols, :] = w.T
    nr_v[tpi] = ns_v[...]
    for q in range(1, tp):
        cp = remote(ns_v, nr_v.at[tpi], n_s.at[q], n_r.at[q], {"tp": lax.rem(tpi + q, tp)})
        cp.start()
        sends.append(cp)

    for q in range(1, tp):
        frm = lax.rem(tpi + tp - q, tp)
        remote(gp_v.at[tpi], gp_v.at[frm], a_s.at[q], a_r.at[q], {"tp": partner}).wait_recv()
    gsum = gp_v[0]
    for j in range(1, tp):
        gsum = gsum + gp_v[j]
    gback_v[0, 0:1, :] = gsum[0:1, :]
    for r in range(1, ep):
        gsum_v[r] = jnp.broadcast_to(gsum[r:r + 1, :], (8, LANES))
        cp = remote(gsum_v.at[r], gback_v.at[r], b_s.at[r], b_r.at[r], {"ep": behind(r)})
        cp.start()
        sends.append(cp)

    norm = jnp.zeros((hidden_units, 1), f32)
    for h in range(CORES):
        for c0 in range(0, half, step):
            cols = slice(h * half + c0, h * half + c0 + step)
            w = dot_nn(tr_v[2], all_v[1, h, :, c0:c0 + step])
            norm = norm + jnp.sum(w * w, axis=1, keepdims=True)
            dw_v[:, cols] = w
    diag = lax.broadcasted_iota(jnp.int32, (hidden_units, hidden_units), 0) == (
        lax.broadcasted_iota(jnp.int32, (hidden_units, hidden_units), 1)
    )
    dn_ref[...] = jnp.sum(jnp.where(diag, norm, 0.0), axis=0, keepdims=True)

    acc = None
    for q in order:
        part = None
        for r in range(ep):
            rs = pl.ds(r * cap, cap)
            if r > 0:
                remote(
                    xs_v.at[q, rs, :], ret_v.at[q, rs, :],
                    x_s.at[q, r], x_r.at[q, r], {"ep": behind(r)},
                ).wait_recv()
            term = dot_nn(pt_v[r][:, :cap], ret_v[q, r * cap:(r + 1) * cap, :])
            part = term if part is None else part + term
        if q == 0:
            acc = part
        else:
            zs_v[q] = part.astype(bf16)
            to = lax.rem(chip + q, nz) * CORES + core
            cp = remote(zs_v.at[q], zr_v.at[q], z_s.at[q], z_r.at[q], {"tp": to})
            cp.start()
            sends.append(cp)

    res = [jnp.zeros((1, rows), f32), jnp.zeros((1, rows), f32)]
    for r in range(ep):
        if r > 0:
            remote(
                gsum_v.at[r], gback_v.at[r], b_s.at[r], b_r.at[r], {"ep": behind(r)}
            ).wait_recv()
        col = jnp.sum(jnp.where(square, gback_v[r, 0:1, :], 0.0), axis=1, keepdims=True)
        val = jnp.sum(pk_v[r].astype(f32) * col, axis=0, keepdims=True)
        for k in range(2):
            res[k] = res[k] + jnp.where(rel[k:k + 1, :] == r, val, 0.0)
    dgate_ref[0:1, :] = res[0]
    dgate_ref[1:2, :] = res[1]

    for q in range(1, tp):
        frm = lax.rem(tpi + tp - q, tp)
        remote(ns_v, nr_v.at[frm], n_s.at[q], n_r.at[q], {"tp": partner}).wait_recv()
    norms = nr_v[0]
    for j in range(1, tp):
        norms = norms + nr_v[j]
    gn_ref[...] = norms[0:1, :]
    ln_ref[...] = norms[1:2, :]

    for q in range(1, nz):
        remote(zs_v.at[q], zr_v.at[q], z_s.at[q], z_r.at[q], {"tp": partner}).wait_recv()
        acc = acc + zr_v[q].astype(f32)
    dtok_ref[...] = acc.astype(bf16)

    for cp in sends:
        cp.wait_send()


def write_out(*refs):
    count = (len(refs) - 1) // 2
    copies = [
        pltpu.make_async_copy(refs[i], refs[count + i], refs[-1].at[i]) for i in range(count)
    ]
    for cp in copies:
        cp.start()
    for cp in copies:
        cp.wait()


def shards(tokens, routes, gates, cotangent, w_glu, w_lin, w_down):
    ep = lax.axis_size("ep")
    tp = lax.axis_size("tp")
    rows, top = routes.shape
    width = tokens.shape[1]
    units = w_glu.shape[2]
    cap = 3 * rows * top // (2 * ep)
    cap = -(-cap // 16) * 16
    slots = ep * cap
    half = width // CORES
    own = width // tp
    nz = tp // CORES
    vm = pl.BlockSpec(memory_space=pltpu.VMEM)
    hbm = pl.BlockSpec(memory_space=pltpu.HBM)
    dma = pltpu.SemaphoreType.DMA
    erows = max(8, ep)
    V = pltpu.VMEM
    out_shape = (
        jax.ShapeDtypeStruct((rows, own), bf16),
        jax.ShapeDtypeStruct((top, rows), f32),
        jax.ShapeDtypeStruct((width, units), f32),
        jax.ShapeDtypeStruct((width, units), f32),
        jax.ShapeDtypeStruct((units, width), f32),
        jax.ShapeDtypeStruct((1, width), f32),
        jax.ShapeDtypeStruct((1, width), f32),
        jax.ShapeDtypeStruct((1, units), f32),
    )
    outs = pl.pallas_call(
        functools.partial(kernel, ep, tp, cap),
        out_shape=out_shape,
        in_specs=[hbm] * 7,
        out_specs=(vm,) * 8,
        scratch_shapes=[
            V((rows, width), bf16),
            V((top, rows), jnp.int32),
            V((top, rows), f32),
            V((rows, width), bf16),
            V((width, units), bf16),
            V((width, units), bf16),
            V((units, width), bf16),
            V((ep, rows, LANES), bf16),
            V((ep, rows, LANES), bf16),
            V((2, ep, cap, half), bf16),
            V((2, CORES, slots, half), bf16),
            V((ep, 8, LANES), f32),
            V((ep, 8, LANES), f32),
            V((3, slots, units), bf16),
            V((3, units, slots), bf16),
            V((nz, slots, own), bf16),
            V((nz, slots, own), bf16),
            V((nz, slots, own), f32),
            V((nz, slots, own), bf16),
            V((nz, slots, own), bf16),
            V((nz, rows, own), bf16),
            V((nz, rows, own), bf16),
            V((tp, erows, LANES), f32),
            V((ep, 8, LANES), f32),
            V((ep, 8, LANES), f32),
            V((2, width), f32),
            V((tp, 2, width), f32),
            dma((3, ep)), dma((3, ep)), dma((2, ep)), dma((2, ep)), dma((ep,)), dma((ep,)),
            dma((5, ep)), dma((5, ep)),
            dma((nz,)), dma((nz,)), dma((nz, ep)), dma((nz, ep)), dma((nz,)), dma((nz,)),
            dma((tp,)), dma((tp,)), dma((ep,)), dma((ep,)), dma((tp,)), dma((tp,)), dma((7,)),
        ],
        compiler_params=pltpu.CompilerParams(
            collective_id=0, has_side_effects=True, vmem_limit_bytes=28 * 1024 * 1024
        ),
    )(*(pltpu.with_memory_space_constraint(x, pltpu.HBM) for x in (
        tokens, routes.T, gates.T, cotangent, w_glu[0], w_lin[0], w_down[0]
    )))
    outs = pl.pallas_call(
        write_out,
        out_shape=out_shape,
        in_specs=[vm] * len(out_shape),
        out_specs=(hbm,) * len(out_shape),
        scratch_shapes=[dma((len(out_shape),))],
        compiler_params=pltpu.CompilerParams(vmem_limit_bytes=28 * 1024 * 1024),
    )(*outs)
    d_tokens, d_gates, gw, lw, dw, gn, ln, dn = outs
    return (d_tokens, d_gates.T, gw[None], lw[None], dw[None], gn, ln, dn)


def solution(mesh):
    in_specs = (
        P("ep", None),
        P("ep", None),
        P("ep", None),
        P("ep", None),
        P("ep", None, "tp"),
        P("ep", None, "tp"),
        P("ep", "tp", None),
    )
    out_specs = (
        P("ep", "tp"),
        P("ep", None),
        P("ep", None, "tp"),
        P("ep", None, "tp"),
        P("ep", "tp", None),
        P("ep", None),
        P("ep", None),
        P("ep", "tp"),
    )
    return jax.shard_map(shards, mesh=mesh, in_specs=in_specs, out_specs=out_specs, check_vma=False)
```

profile of v0, /device:TPU:0, one launch (start us, length us, event | category | flops | bytes accessed | tf_op | source)
XLA Modules:
  0.0 41.4 jit_solution(9500275171075646377)
XLA Ops:
  0.6 39.0 %shard_map.134 = (bf16[128,256]{1,0:T(8,128)(2,1)S(1)}, f32[2,128]{1,0:T(2,128)S(1)}, f32[2048,128]{1,0:T(8,128)S(1)}, f32[2048,128]{1,0:T(8,128)S(1)}, f32[128,...) custom-call(bf16[128,2048]{1,0:T(8,128)(2,1)} %tok_hbm.1, ...), custom_call_target="tpu_custom_call" | custom-call | tf_op jit(solution)/shard_map/pallas_call | solution.py:404
  39.7 1.8 %shard_map.135 = (bf16[128,256]{1,0:T(8,128)(2,1)}, f32[2,128]{1,0:T(2,128)}, f32[2048,128]{1,0:T(8,128)}, f32[2048,128]{1,0:T(8,128)}, f32[128,2048]{1,0:T(8,12...) custom-call(bf16[128,256]{1,0:T(8,128)(2,1)S(1)} %get-tuple-element.24.refs_0_, ...), custom_call_target="tpu_custom_call" | custom-call | tf_op jit(solution)/shard_map/pallas_call | solution.py:448
where the time goes:
time: 41.6 us; the launch traced here: 41.4 us
  Pallas kernels  40.8 us (98%)
  between operations  0.64 us (2%)
    pallas_call x1, Pallas kernels, shards(): pl.pallas_call(functools.partial(kernel, ep, tp, cap), out_shape=out_shap...  39 us
    pallas_call x1, Pallas kernels, shards(): pl.pallas_call(write_out, out_shape=out_shape, in_specs=[vm] * len(out_sh...  1.77 us

commit v1 on v0

v1 whole, which is shorter than its diff:
```python
import functools

import jax
import jax.numpy as jnp
from jax import lax
from jax.experimental import pallas as pl
from jax.experimental.pallas import tpu as pltpu
from jax.sharding import PartitionSpec as P

clamp_limit = 7.0
sigmoid_scale = 1.702
MESH = pl.DeviceIdType.MESH
LANES = 128
CORES = 2
SLABS = 2
f32 = jnp.float32
bf16 = jnp.bfloat16


def dot_nn(a, b):
    return lax.dot_general(a, b, (((1,), (0,)), ((), ())), preferred_element_type=f32)


def dot_nt(a, b):
    return lax.dot_general(a, b, (((1,), (1,)), ((), ())), preferred_element_type=f32)


def flip(index, mask):
    bit = 1
    while bit <= mask:
        if mask & bit:
            index = index + bit - 2 * bit * lax.rem(lax.div(index, bit), 2)
        bit = 2 * bit
    return index


def clamp_backward(glu_pre, lin_pre, back_proj, gate_col):
    glu_clip = jnp.minimum(glu_pre, clamp_limit)
    lin_clip = jnp.clip(lin_pre, -clamp_limit, clamp_limit)
    sig_val = jax.nn.sigmoid(sigmoid_scale * glu_clip)
    glu_act = glu_clip * sig_val
    hidden = glu_act * (lin_clip + 1.0)
    hid_grad = gate_col * back_proj
    act_slope = sig_val + sigmoid_scale * glu_clip * sig_val * (1.0 - sig_val)
    glu_grad = jnp.where(glu_pre < clamp_limit, hid_grad * (lin_clip + 1.0) * act_slope, 0.0)
    lin_grad = jnp.where(jnp.abs(lin_pre) < clamp_limit, hid_grad * glu_act, 0.0)
    return hidden, glu_grad.astype(bf16), lin_grad.astype(bf16)


def piece_list(half):
    narrow = half // 8
    return (
        (1, 0, half // 2, True),
        (0, 0, narrow, True),
        (0, 2 * narrow, half - 2 * narrow, False),
    )


def semaphores(ep, nz, pieces):
    keys = [("load", i) for i in range(7)]
    keys += [(k, 0) for k in ("gs", "ps", "xs", "zs", "as", "bs", "ns")]
    keys += [(k, 0) for k in ("gr", "zr", "ar", "br", "nr")]
    keys += [("ys", a) for a in range(2)]
    for i, piece in enumerate(pieces):
        keys.append(("ds", i))
        if piece[3]:
            keys.append(("hs", i))
        for s in range(SLABS):
            if piece[3]:
                keys += [("dr", i, s, r) for r in range(1, ep)]
                keys.append(("hr", i, s))
            else:
                keys.append(("dr", i, s))
    for s in range(SLABS):
        keys += [("yr", a, s) for a in range(2)]
    for q in range(nz):
        keys.append(("xr", q))
        keys += [("pr", q, s) for s in range(1 + SLABS)]
    return {key: i for i, key in enumerate(keys)}


def kernel(
    ep, tp, cap,
    tok_hbm, routes_hbm, gates_hbm, cot_hbm, wg_hbm, wl_hbm, wd_hbm,
    dtok_ref, dgate_ref, gw_v, lw_v, dw_v, gn_ref, ln_ref, dn_ref,
    tok_ref, routes_ref, gates_ref, cot_ref, wg_ref, wl_ref, wcat_ref, wd_ref,
    pt_v, pk_v, snd_v, all_v, gsnd_v, grow_v, bf_v, hg_v, tr_v,
    ps_v, pr_v, mine_v, xs_v, ret_v, zs_v, zr_v,
    gp_v, gsum_v, gback_v, ns_v, nr_v, sem_v,
):
    me = lax.axis_index("ep")
    tpi = lax.axis_index("tp")
    nz = tp // CORES
    core = lax.rem(tpi, CORES)
    chip = lax.div(tpi, CORES)
    other = 1 - core
    partner = chip * CORES + other
    rows = tok_ref.shape[0]
    width = tok_ref.shape[1]
    units = wd_ref.shape[0]
    half = width // CORES
    own = width // tp
    odd = lax.rem(chip, 2)
    beside = flip(chip, 1) * CORES + core
    span = cap // SLABS
    slab = (ep - 1) * span
    far = SLABS * slab
    pieces = piece_list(half)
    table = semaphores(ep, nz, pieces)

    def sem(*key):
        return sem_v.at[table[key]]

    aligned = units % LANES == 0
    loads = []
    for i, (src, dst) in enumerate((
        (routes_hbm, routes_ref), (gates_hbm, gates_ref), (cot_hbm, cot_ref), (tok_hbm, tok_ref),
        (wg_hbm, wcat_ref.at[:, pl.ds(0, units)] if aligned else wg_ref),
        (wl_hbm, wcat_ref.at[:, pl.ds(units, units)] if aligned else wl_ref),
        (wd_hbm, wd_ref),
    )):
        cp = pltpu.make_async_copy(src, dst, sem("load", i))
        cp.start()
        loads.append(cp)

    barrier = pltpu.get_barrier_semaphore()
    for r in range(1, ep):
        pl.semaphore_signal(barrier, inc=1, device_id={"ep": flip(me, r)}, device_id_type=MESH)
    for q in range(1, tp):
        pl.semaphore_signal(
            barrier, inc=1, device_id={"tp": lax.rem(tpi + q, tp)}, device_id_type=MESH
        )

    def remote(src, dst, ss, rs, where):
        return pltpu.make_async_remote_copy(
            src_ref=src, dst_ref=dst, send_sem=ss, recv_sem=rs,
            device_id=where, device_id_type=MESH,
        )

    def arrived(ref, *key):
        remote(ref, ref, sem(*key), sem(*key), {"tp": partner}).wait_recv()

    def sent(ref, *key):
        remote(ref, ref, sem(*key), sem(*key), {"tp": partner}).wait_send()

    loads[0].wait()
    loads[1].wait()
    rel = jnp.bitwise_xor(routes_ref[...], me)
    erows = gp_v.shape[1]
    sub = lax.broadcasted_iota(jnp.int32, (erows, rows), 0)
    first, second = sub == rel[0:1, :], sub == rel[1:2, :]
    mask = jnp.where(first, 1.0, 0.0) + jnp.where(second, 1.0, 0.0)
    gate_of = jnp.where(first, gates_ref[0:1, :], 0.0) + jnp.where(second, gates_ref[1:2, :], 0.0)
    before = lax.broadcasted_iota(jnp.int32, (rows, rows), 0) < lax.broadcasted_iota(
        jnp.int32, (rows, rows), 1
    )
    rank = dot_nn(mask.astype(bf16), jnp.where(before, 1.0, 0.0).astype(bf16))
    place = jnp.where(mask > 0.5, rank, -1.0)
    slot_at = lax.broadcasted_iota(jnp.int32, (LANES, rows), 0).astype(f32)
    hits = [jnp.where(slot_at == place[r:r + 1, :], 1.0, 0.0) for r in range(ep)]
    outgoing = [
        jnp.concatenate([hits[r][s * span:(s + 1) * span, :] for r in range(1, ep)], axis=0)
        for s in range(SLABS)
    ]
    picks = [x.astype(bf16) for x in outgoing]
    square = lax.broadcasted_iota(jnp.int32, (LANES, LANES), 0) == lax.broadcasted_iota(
        jnp.int32, (LANES, LANES), 1
    )
    swapped = [i for i, piece in enumerate(pieces) if piece[3]]
    refs = (tok_ref, cot_ref)

    def window(i, whose):
        a, off, w, shared = pieces[i]
        if shared:
            off = off + whose * w
        return a, (pl.ds(pl.multiple_of(off, LANES), w) if shared else pl.ds(off, w))

    def block(s, r):
        return pl.ds(cap + s * slab + (r - 1) * span, span)

    def area(i, at, whose):
        a, cols = window(i, whose)
        return all_v.at[a, core, at, cols]

    def relay(i, s, whose):
        a = pieces[i][0]
        at = area(i, pl.ds(cap + s * slab, slab), whose)
        remote(at, at, sem("ys", a), sem("yr", a, s), {"tp": partner}).start()

    loads[2].wait()
    loads[3].wait()
    waited = False
    for s in range(SLABS):
        for i in range(len(pieces)):
            a, off, w, shared = pieces[i]
            cols = window(i, odd)[1]
            begin = core * half + off + (odd * w if shared else 0)
            src_cols = pl.ds(pl.multiple_of(begin, LANES), w)
            snd_v[a, s * slab:(s + 1) * slab, cols] = dot_nn(
                picks[s], refs[a][:, src_cols]
            ).astype(bf16)
            if not waited:
                pl.semaphore_wait(barrier, ep - 1 + tp - 1)
                waited = True
            for r in reversed(range(1, ep)):
                key = ("dr", i, s, r) if shared else ("dr", i, s)
                remote(
                    snd_v.at[a, pl.ds(s * slab + (r - 1) * span, span), cols],
                    area(i, block(s, r), odd), sem("ds", i), sem(*key), {"ep": flip(me, r)},
                ).start()
    for r in range(ep):
        col = jnp.sum(hits[r] * gate_of[r:r + 1, :], axis=1, keepdims=True)
        row = jnp.sum(jnp.where(square, col, 0.0), axis=0, keepdims=True)
        if r == 0:
            grow_v[0] = jnp.broadcast_to(row, (8, LANES))
        else:
            gsnd_v[r] = jnp.broadcast_to(row, (8, LANES))
            remote(
                gsnd_v.at[r], grow_v.at[r], sem("gs", 0), sem("gr", 0), {"ep": flip(me, r)}
            ).start()
    home = hits[0][:cap, :].astype(bf16)
    for a, ref in ((0, tok_ref), (1, cot_ref)):
        for h in range(CORES):
            all_v[a, h, 0:cap, :] = dot_nn(home, ref[:, h * half:(h + 1) * half]).astype(bf16)
    for r in range(ep):
        pk_v[r] = hits[r].astype(bf16)
    pt_v[...] = jnp.concatenate([hits[0][:cap, :]] + outgoing, axis=0).T.astype(bf16)

    gp_v[tpi] = jnp.zeros(gp_v.shape[1:], f32)

    def forward(at, count, blocks, shift, ready):
        eye = lax.broadcasted_iota(jnp.int32, (count, LANES), 0) + shift == (
            lax.broadcasted_iota(jnp.int32, (count, LANES), 1)
        )
        rs = slice(at, at + count * len(blocks))
        n = rs.stop - rs.start
        ready(1)
        back = jnp.zeros((n, units), f32)
        for h in range(CORES):
            back = back + dot_nt(all_v[1, h, rs, :], wd_ref[:, h * half:(h + 1) * half])
        gate_col = jnp.concatenate([
            jnp.sum(jnp.where(eye, grow_v[r, 0:1, :], 0.0), axis=1, keepdims=True)
            for r in blocks
        ], axis=0)
        ready(0)
        pre = jnp.zeros((n, 2 * units), f32)
        for h in range(CORES):
            pre = pre + dot_nn(all_v[0, h, rs, :], wcat_ref[h * half:(h + 1) * half, :])
        hidden, glu_bf, lin_bf = clamp_backward(
            pre[:, 0:units], pre[:, units:2 * units], back, gate_col
        )
        part = jnp.sum(back * hidden, axis=1, keepdims=True)
        bf_v[rs, 0:units] = glu_bf
        bf_v[rs, units:2 * units] = lin_bf
        hg_v[rs, :] = (gate_col * hidden).astype(bf16)
        for k, r in enumerate(blocks):
            line = jnp.sum(
                jnp.where(eye, part[k * count:(k + 1) * count, :], 0.0), axis=0, keepdims=True
            )
            gp_v[tpi, r:r + 1, :] = gp_v[tpi, r:r + 1, :] + line

    order = list(reversed(range(1, nz))) + [0]

    def input_cols(k, which, rs):
        at = pl.ds(pl.multiple_of((flip(chip, k) * CORES + which) * own, own), own)
        return dot_nt(bf_v[rs, :], wcat_ref[at, :])

    def give(b, rs):
        at = pl.ds(rs.start, rs.stop - rs.start)
        for q in order:
            ps_v[q, rs, :] = input_cols(q, other, rs).astype(bf16)
            remote(
                ps_v.at[q, at, :], pr_v.at[q, at, :], sem("ps", 0), sem("pr", q, b),
                {"tp": partner},
            ).start()
        for q in order:
            mine_v[q, rs, :] = input_cols(q, core, rs)

    def take(b, rs):
        at = pl.ds(rs.start, rs.stop - rs.start)
        for q in order:
            arrived(pr_v.at[q, at, :], "pr", q, b)
            total = (mine_v[q, rs, :] + pr_v[q, rs, :].astype(f32)).astype(bf16)
            if b == 0:
                ret_v[q, rs, :] = total
                continue
            xs_v[q, rs, :] = total
            for r in reversed(range(1, ep)):
                where = block(b - 1, r)
                remote(
                    xs_v.at[q, where, :], ret_v.at[q, where, :],
                    sem("xs", 0), sem("xr", q), {"ep": flip(me, r)},
                ).start()

    def slab_rows(s):
        return slice(cap + s * slab, cap + (s + 1) * slab)

    def pass_shared(s):
        for i in swapped:
            for r in reversed(range(1, ep)):
                at = area(i, block(s, r), odd)
                arrived(at, "dr", i, s, r)
                remote(at, at, sem("hs", i), sem("hr", i, s), {"tp": beside}).start()
            relay(i, s, odd)

    def pass_rest(s):
        whole = pl.ds(cap + s * slab, slab)
        for i in range(len(pieces)):
            if i in swapped:
                arrived(area(i, whole, 1 - odd), "hr", i, s)
                relay(i, s, 1 - odd)
        for i in range(len(pieces)):
            if i not in swapped:
                arrived(area(i, whole, odd), "dr", i, s)
                relay(i, s, odd)

    def landed(s):
        def ready(a):
            arrived(all_v.at[a, other, pl.ds(cap + s * slab, slab), :], "yr", a, s)
        return ready

    home_rows = slice(0, cap)
    remote_blocks = list(range(1, ep))
    pass_shared(0)
    for cp in loads[4:]:
        cp.wait()
    if not aligned:
        wcat_ref[...] = jnp.concatenate([wg_ref[...], wl_ref[...]], axis=1)
    forward(0, cap, [0], 0, lambda a: None)
    give(0, home_rows)
    pass_rest(0)
    arrived(grow_v.at[pl.ds(1, ep - 1)], "gr", 0)
    for s in range(SLABS):
        forward(cap + s * slab, span, remote_blocks, s * span, landed(s))
        give(1 + s, slab_rows(s))
        if s == 0:
            take(0, home_rows)
        if s + 1 < SLABS:
            pass_shared(s + 1)
        take(1 + s, slab_rows(s))
        if s + 1 < SLABS:
            pass_rest(s + 1)

    for q in range(1, tp):
        remote(
            gp_v.at[tpi], gp_v.at[tpi], sem("as", 0), sem("ar", 0),
            {"tp": lax.rem(tpi + q, tp)},
        ).start()

    tr_v[0:2 * units, :] = bf_v[...].astype(f32).T.astype(bf16)
    tr_v[2 * units:3 * units, :] = hg_v[...].astype(f32).T.astype(bf16)
    step = min(512, half)
    for h in range(CORES):
        for c0 in range(0, half, step):
            cols = slice(h * half + c0, h * half + c0 + step)
            w = dot_nn(tr_v[0:2 * units, :], all_v[0, h, :, c0:c0 + step])
            for n, w_v in enumerate((gw_v, lw_v)):
                wn = w[n * units:(n + 1) * units, :]
                ns_v[n:n + 1, cols] = jnp.sum(wn * wn, axis=0, keepdims=True)
                w_v[cols, :] = wn.T
    nr_v[tpi] = ns_v[...]
    for q in range(1, tp):
        remote(
            ns_v, nr_v.at[tpi], sem("ns", 0), sem("nr", 0), {"tp": lax.rem(tpi + q, tp)}
        ).start()

    arrived(gp_v.at[pl.ds(1, tp - 1)], "ar", 0)
    gsum = gp_v[0]
    for j in range(1, tp):
        gsum = gsum + gp_v[j]
    gback_v[0, 0:1, :] = gsum[0:1, :]
    for r in range(1, ep):
        gsum_v[r] = jnp.broadcast_to(gsum[r:r + 1, :], (8, LANES))
        remote(
            gsum_v.at[r], gback_v.at[r], sem("bs", 0), sem("br", 0), {"ep": flip(me, r)}
        ).start()

    norm = jnp.zeros((units, 1), f32)
    for h in range(CORES):
        for c0 in range(0, half, step):
            cols = slice(h * half + c0, h * half + c0 + step)
            w = dot_nn(tr_v[2 * units:3 * units, :], all_v[1, h, :, c0:c0 + step])
            norm = norm + jnp.sum(w * w, axis=1, keepdims=True)
            dw_v[:, cols] = w
    diag = lax.broadcasted_iota(jnp.int32, (units, units), 0) == (
        lax.broadcasted_iota(jnp.int32, (units, units), 1)
    )
    dn_ref[...] = jnp.sum(jnp.where(diag, norm, 0.0), axis=0, keepdims=True)

    acc = None
    for q in order:
        arrived(ret_v.at[q, pl.ds(cap, far), :], "xr", q)
        part = dot_nn(pt_v[...], ret_v[q])
        if q == 0:
            acc = part
        else:
            zs_v[q] = part.astype(bf16)
            remote(
                zs_v.at[q], zr_v.at[q], sem("zs", 0), sem("zr", 0),
                {"tp": flip(chip, q) * CORES + core},
            ).start()

    arrived(gback_v.at[pl.ds(1, ep - 1)], "br", 0)
    res = [jnp.zeros((1, rows), f32), jnp.zeros((1, rows), f32)]
    for r in range(ep):
        col = jnp.sum(jnp.where(square, gback_v[r, 0:1, :], 0.0), axis=1, keepdims=True)
        val = jnp.sum(pk_v[r].astype(f32) * col, axis=0, keepdims=True)
        for k in range(2):
            res[k] = res[k] + jnp.where(rel[k:k + 1, :] == r, val, 0.0)
    dgate_ref[0:1, :] = res[0]
    dgate_ref[1:2, :] = res[1]

    arrived(nr_v.at[pl.ds(1, tp - 1)], "nr", 0)
    norms = nr_v[0]
    for j in range(1, tp):
        norms = norms + nr_v[j]
    gn_ref[...] = norms[0:1, :]
    ln_ref[...] = norms[1:2, :]

    if nz > 1:
        arrived(zr_v.at[pl.ds(1, nz - 1)], "zr", 0)
    for q in range(1, nz):
        acc = acc + zr_v[q].astype(f32)
    dtok_ref[...] = acc.astype(bf16)

    remote_rows = pl.ds(cap, far)
    for i in range(len(pieces)):
        a, cols = window(i, odd)
        sent(snd_v.at[a, :, cols], "ds", i)
        if i in swapped:
            sent(area(i, remote_rows, odd), "hs", i)
    for a in range(2):
        sent(all_v.at[a, core, remote_rows, :], "ys", a)
    sent(gsnd_v.at[pl.ds(1, ep - 1)], "gs", 0)
    sent(ps_v, "ps", 0)
    sent(xs_v.at[:, remote_rows, :], "xs", 0)
    if nz > 1:
        sent(zs_v.at[pl.ds(1, nz - 1)], "zs", 0)
    sent(gp_v.at[pl.ds(1, tp - 1)], "as", 0)
    sent(gsum_v.at[pl.ds(1, ep - 1)], "bs", 0)
    sent(nr_v.at[pl.ds(1, tp - 1)], "ns", 0)


def write_out(*refs):
    count = (len(refs) - 1) // 2
    copies = [
        pltpu.make_async_copy(refs[i], refs[count + i], refs[-1].at[i]) for i in range(count)
    ]
    for cp in copies:
        cp.start()
    for cp in copies:
        cp.wait()


def shards(tokens, routes, gates, cotangent, w_glu, w_lin, w_down):
    ep = lax.axis_size("ep")
    tp = lax.axis_size("tp")
    rows, top = routes.shape
    width = tokens.shape[1]
    units = w_glu.shape[2]
    cap = 3 * rows * top // (2 * ep)
    cap = -(-cap // (16 * SLABS)) * (16 * SLABS)
    slots = ep * cap
    half = width // CORES
    own = width // tp
    nz = tp // CORES
    vm = pl.BlockSpec(memory_space=pltpu.VMEM)
    hbm = pl.BlockSpec(memory_space=pltpu.HBM)
    dma = pltpu.SemaphoreType.DMA
    erows = max(8, ep)
    V = pltpu.VMEM
    out_shape = (
        jax.ShapeDtypeStruct((rows, own), bf16),
        jax.ShapeDtypeStruct((top, rows), f32),
        jax.ShapeDtypeStruct((width, units), f32),
        jax.ShapeDtypeStruct((width, units), f32),
        jax.ShapeDtypeStruct((units, width), f32),
        jax.ShapeDtypeStruct((1, width), f32),
        jax.ShapeDtypeStruct((1, width), f32),
        jax.ShapeDtypeStruct((1, units), f32),
    )
    outs = pl.pallas_call(
        functools.partial(kernel, ep, tp, cap),
        out_shape=out_shape,
        in_specs=[hbm] * 7,
        out_specs=(vm,) * 8,
        scratch_shapes=[
            V((rows, width), bf16),
            V((top, rows), jnp.int32),
            V((top, rows), f32),
            V((rows, width), bf16),
            V((width, units) if units % LANES else (16, LANES), bf16),
            V((width, units) if units % LANES else (16, LANES), bf16),
            V((width, 2 * units), bf16),
            V((units, width), bf16),
            V((rows, slots), bf16),
            V((ep, LANES, rows), bf16),
            V((2, slots - cap, half), bf16),
            V((2, CORES, slots, half), bf16),
            V((ep, 8, LANES), f32),
            V((ep, 8, LANES), f32),
            V((slots, 2 * units), bf16),
            V((slots, units), bf16),
            V((3 * units, slots), bf16),
            V((nz, slots, own), bf16),
            V((nz, slots, own), bf16),
            V((nz, slots, own), f32),
            V((nz, slots, own), bf16),
            V((nz, slots, own), bf16),
            V((nz, rows, own), bf16),
            V((nz, rows, own), bf16),
            V((tp, erows, LANES), f32),
            V((ep, 8, LANES), f32),
            V((ep, 8, LANES), f32),
            V((2, width), f32),
            V((tp, 2, width), f32),
            dma((len(semaphores(ep, nz, piece_list(half))),)),
        ],
        compiler_params=pltpu.CompilerParams(
            collective_id=0, has_side_effects=True, vmem_limit_bytes=28 * 1024 * 1024
        ),
    )(*(pltpu.with_memory_space_constraint(x, pltpu.HBM) for x in (
        tokens, routes.T, gates.T, cotangent, w_glu[0], w_lin[0], w_down[0]
    )))
    outs = pl.pallas_call(
        write_out,
        out_shape=out_shape,
        in_specs=[vm] * len(out_shape),
        out_specs=(hbm,) * len(out_shape),
        scratch_shapes=[dma((len(out_shape),))],
        compiler_params=pltpu.CompilerParams(vmem_limit_bytes=28 * 1024 * 1024),
    )(*outs)
    d_tokens, d_gates, gw, lw, dw, gn, ln, dn = outs
    return (d_tokens, d_gates.T, gw[None], lw[None], dw[None], gn, ln, dn)


def solution(mesh):
    in_specs = (
        P("ep", None),
        P("ep", None),
        P("ep", None),
        P("ep", None),
        P("ep", None, "tp"),
        P("ep", None, "tp"),
        P("ep", "tp", None),
    )
    out_specs = (
        P("ep", "tp"),
        P("ep", None),
        P("ep", None, "tp"),
        P("ep", None, "tp"),
        P("ep", "tp", None),
        P("ep", None),
        P("ep", None),
        P("ep", "tp"),
    )
    return jax.shard_map(shards, mesh=mesh, in_specs=in_specs, out_specs=out_specs, check_vma=False)
```

time: 41.6 us -> 46.1 us (1.11)
  Pallas kernels: 40.8 us -> 45.3 us
    pallas_call x1, Pallas kernels: 39 us -> 43.6 us  [shards(): pl.pallas_call(functools.partial(kernel, ep, tp, cap), out_shape=out_shap...]
where the time goes in v1:
time: 46.1 us; the launch traced here: 46 us
  Pallas kernels  45.3 us (98%)
  between operations  0.64 us (1%)
    pallas_call x1, Pallas kernels, shards(): pl.pallas_call(functools.partial(kernel, ep, tp, cap), out_shape=out_shap...  43.6 us
    pallas_call x1, Pallas kernels, shards(): pl.pallas_call(write_out, out_shape=out_shape, in_specs=[vm] * len(out_sh...  1.77 us

profile of v1, /device:TPU:0, one launch (start us, length us, event | category | flops | bytes accessed | tf_op | source)
XLA Modules:
  0.0 46.0 jit_solution(9758666609392300995)
XLA Ops:
  0.6 43.6 %shard_map.134 = (bf16[128,256]{1,0:T(8,128)(2,1)S(1)}, f32[2,128]{1,0:T(2,128)S(1)}, f32[2048,128]{1,0:T(8,128)S(1)}, f32[2048,128]{1,0:T(8,128)S(1)}, f32[128,...) custom-call(bf16[128,2048]{1,0:T(8,128)(2,1)} %tok_hbm.1, ...), custom_call_target="tpu_custom_call" | custom-call | tf_op jit(solution)/shard_map/pallas_call | solution.py:482
  44.2 1.8 %shard_map.135 = (bf16[128,256]{1,0:T(8,128)(2,1)}, f32[2,128]{1,0:T(2,128)}, f32[2048,128]{1,0:T(8,128)}, f32[2048,128]{1,0:T(8,128)}, f32[128,2048]{1,0:T(8,12...) custom-call(bf16[128,256]{1,0:T(8,128)(2,1)S(1)} %get-tuple-element.24.refs_0_, ...), custom_call_target="tpu_custom_call" | custom-call | tf_op jit(solution)/shard_map/pallas_call | solution.py:525

commit v2 on v1

--- a/solution.py
+++ b/solution.py
@@ -12,7 +12,8 @@
 MESH = pl.DeviceIdType.MESH
 LANES = 128
 CORES = 2
-SLABS = 2
+SHARE = 3
+FLIGHT = 6
 f32 = jnp.float32
 bf16 = jnp.bfloat16
 
@@ -47,35 +48,39 @@
     return hidden, glu_grad.astype(bf16), lin_grad.astype(bf16)
 
 
+def slab_cuts(cap):
+    first = min(-(-2 * cap // 48) * 16, cap - 16)
+    return (first, cap - first)
+
+
 def piece_list(half):
-    narrow = half // 8
-    return (
-        (1, 0, half // 2, True),
-        (0, 0, narrow, True),
-        (0, 2 * narrow, half - 2 * narrow, False),
-    )
-
-
-def semaphores(ep, nz, pieces):
+    unit = half // 8
+    early = tuple((1, 2 * k * unit, unit, True) for k in range(4)) + (
+        (0, 0, unit, True),
+    ) + tuple((0, (2 + 2 * k) * unit, 2 * unit, False) for k in range(3))
+    late = (
+        (1, 0, SHARE * unit, True),
+        (1, 2 * SHARE * unit, half - 2 * SHARE * unit, False),
+        (0, 0, half // 2, False),
+        (0, half // 2, half // 2, False),
+    )
+    return (early, late)
+
+
+def semaphores(ep, nz, plan):
     keys = [("load", i) for i in range(7)]
-    keys += [(k, 0) for k in ("gs", "ps", "xs", "zs", "as", "bs", "ns")]
-    keys += [(k, 0) for k in ("gr", "zr", "ar", "br", "nr")]
-    keys += [("ys", a) for a in range(2)]
-    for i, piece in enumerate(pieces):
-        keys.append(("ds", i))
-        if piece[3]:
-            keys.append(("hs", i))
-        for s in range(SLABS):
+    keys += [(k, 0) for k in ("gs", "ps", "xs", "zs", "as", "bs", "ns", "ds", "hs", "ys")]
+    keys += [(k, 0) for k in ("gr", "ar", "br", "nr")]
+    for s, pieces in enumerate(plan):
+        for i, piece in enumerate(pieces):
+            keys.append(("dr", s, i))
             if piece[3]:
-                keys += [("dr", i, s, r) for r in range(1, ep)]
-                keys.append(("hr", i, s))
-            else:
-                keys.append(("dr", i, s))
-    for s in range(SLABS):
-        keys += [("yr", a, s) for a in range(2)]
+                keys.append(("hr", s, i))
+        keys += [("yr", s, a) for a in range(2)]
+        keys.append(("zr", s))
     for q in range(nz):
-        keys.append(("xr", q))
-        keys += [("pr", q, s) for s in range(1 + SLABS)]
+        keys += [("pr", q, b) for b in range(1 + len(plan))]
+        keys += [("xr", q, s) for s in range(len(plan))]
     return {key: i for i, key in enumerate(keys)}
 
 
@@ -85,7 +90,7 @@
     dtok_ref, dgate_ref, gw_v, lw_v, dw_v, gn_ref, ln_ref, dn_ref,
     tok_ref, routes_ref, gates_ref, cot_ref, wg_ref, wl_ref, wcat_ref, wd_ref,
     pt_v, pk_v, snd_v, all_v, gsnd_v, grow_v, bf_v, hg_v, tr_v,
-    ps_v, pr_v, mine_v, xs_v, ret_v, zs_v, zr_v,
+    ps_v, pr_v, xs_v, ret_v, zs_v, zr_v,
     gp_v, gsum_v, gback_v, ns_v, nr_v, sem_v,
 ):
     me = lax.axis_index("ep")
@@ -102,11 +107,13 @@
     own = width // tp
     odd = lax.rem(chip, 2)
     beside = flip(chip, 1) * CORES + core
-    span = cap // SLABS
-    slab = (ep - 1) * span
-    far = SLABS * slab
-    pieces = piece_list(half)
-    table = semaphores(ep, nz, pieces)
+    cuts = slab_cuts(cap)
+    slabs = [(ep - 1) * n for n in cuts]
+    bases = [cap + sum(slabs[:s]) for s in range(len(cuts))]
+    ranks = [sum(cuts[:s]) for s in range(len(cuts))]
+    far = sum(slabs)
+    plan = piece_list(half)
+    table = semaphores(ep, nz, plan)
 
     def sem(*key):
         return sem_v.at[table[key]]
@@ -159,55 +166,80 @@
     slot_at = lax.broadcasted_iota(jnp.int32, (LANES, rows), 0).astype(f32)
     hits = [jnp.where(slot_at == place[r:r + 1, :], 1.0, 0.0) for r in range(ep)]
     outgoing = [
-        jnp.concatenate([hits[r][s * span:(s + 1) * span, :] for r in range(1, ep)], axis=0)
-        for s in range(SLABS)
+        jnp.concatenate([hits[r][at:at + n, :] for r in range(1, ep)], axis=0)
+        for at, n in zip(ranks, cuts)
     ]
     picks = [x.astype(bf16) for x in outgoing]
     square = lax.broadcasted_iota(jnp.int32, (LANES, LANES), 0) == lax.broadcasted_iota(
         jnp.int32, (LANES, LANES), 1
     )
-    swapped = [i for i, piece in enumerate(pieces) if piece[3]]
     refs = (tok_ref, cot_ref)
 
-    def window(i, whose):
-        a, off, w, shared = pieces[i]
+    def window(s, i, whose):
+        a, off, w, shared = plan[s][i]
         if shared:
-            off = off + whose * w
-        return a, (pl.ds(pl.multiple_of(off, LANES), w) if shared else pl.ds(off, w))
+            return a, pl.ds(pl.multiple_of(off + whose * w, LANES), w)
+        return a, pl.ds(off, w)
 
     def block(s, r):
-        return pl.ds(cap + s * slab + (r - 1) * span, span)
-
-    def area(i, at, whose):
-        a, cols = window(i, whose)
+        return pl.ds(bases[s] + (r - 1) * cuts[s], cuts[s])
+
+    def whole(s):
+        return pl.ds(bases[s], slabs[s])
+
+    def area(s, i, at, whose):
+        a, cols = window(s, i, whose)
         return all_v.at[a, core, at, cols]
 
-    def relay(i, s, whose):
-        a = pieces[i][0]
-        at = area(i, pl.ds(cap + s * slab, slab), whose)
-        remote(at, at, sem("ys", a), sem("yr", a, s), {"tp": partner}).start()
+    def relay(s, i, whose):
+        at = area(s, i, whole(s), whose)
+        remote(at, at, sem("ys", 0), sem("yr", s, plan[s][i][0]), {"tp": partner}).start()
+
+    steps = [(s, i) for s in range(len(cuts)) for i in range(len(plan[s]))]
+    state = {"next": 0, "load": 0, "waited": False}
+
+    def cost(s, i):
+        return cuts[s] * plan[s][i][2]
+
+    def dispatch():
+        s, i = steps[state["next"]]
+        a, off, w, shared = plan[s][i]
+        cols = window(s, i, odd)[1]
+        begin = core * half + off + (odd * w if shared else 0)
+        src_cols = pl.ds(pl.multiple_of(begin, LANES), w)
+        at = bases[s] - cap
+        snd_v[a, at:at + slabs[s], cols] = dot_nn(picks[s], refs[a][:, src_cols]).astype(bf16)
+        if not state["waited"]:
+            pl.semaphore_wait(barrier, ep - 1 + tp - 1)
+            state["waited"] = True
+        for r in reversed(range(1, ep)):
+            remote(
+                snd_v.at[a, pl.ds(at + (r - 1) * cuts[s], cuts[s]), cols],
+                area(s, i, block(s, r), odd), sem("ds", 0), sem("dr", s, i), {"ep": flip(me, r)},
+            ).start()
+        state["next"] += 1
+        state["load"] += cost(s, i)
+
+    def fill():
+        while state["next"] < len(steps) and state["load"] < FLIGHT * cuts[0] * half // 8:
+            dispatch()
+
+    def land(s, i):
+        at = area(s, i, whole(s), odd)
+        arrived(at, "dr", s, i)
+        if plan[s][i][3]:
+            remote(at, at, sem("hs", 0), sem("hr", s, i), {"tp": beside}).start()
+        relay(s, i, odd)
+        state["load"] -= cost(s, i)
+        fill()
+
+    def turn(s, i):
+        arrived(area(s, i, whole(s), 1 - odd), "hr", s, i)
+        relay(s, i, 1 - odd)
 
     loads[2].wait()
     loads[3].wait()
-    waited = False
-    for s in range(SLABS):
-        for i in range(len(pieces)):
-            a, off, w, shared = pieces[i]
-            cols = window(i, odd)[1]
-            begin = core * half + off + (odd * w if shared else 0)
-            src_cols = pl.ds(pl.multiple_of(begin, LANES), w)
-            snd_v[a, s * slab:(s + 1) * slab, cols] = dot_nn(
-                picks[s], refs[a][:, src_cols]
-            ).astype(bf16)
-            if not waited:
-                pl.semaphore_wait(barrier, ep - 1 + tp - 1)
-                waited = True
-            for r in reversed(range(1, ep)):
-                key = ("dr", i, s, r) if shared else ("dr", i, s)
-                remote(
-                    snd_v.at[a, pl.ds(s * slab + (r - 1) * span, span), cols],
-                    area(i, block(s, r), odd), sem("ds", i), sem(*key), {"ep": flip(me, r)},
-                ).start()
+    fill()
     for r in range(ep):
         col = jnp.sum(hits[r] * gate_of[r:r + 1, :], axis=1, keepdims=True)
         row = jnp.sum(jnp.where(square, col, 0.0), axis=0, keepdims=True)
@@ -273,14 +305,13 @@
                 ps_v.at[q, at, :], pr_v.at[q, at, :], sem("ps", 0), sem("pr", q, b),
                 {"tp": partner},
             ).start()
-        for q in order:
-            mine_v[q, rs, :] = input_cols(q, core, rs)
 
     def take(b, rs):
         at = pl.ds(rs.start, rs.stop - rs.start)
         for q in order:
+            mine = input_cols(q, core, rs)
             arrived(pr_v.at[q, at, :], "pr", q, b)
-            total = (mine_v[q, rs, :] + pr_v[q, rs, :].astype(f32)).astype(bf16)
+            total = (mine + pr_v[q, rs, :].astype(f32)).astype(bf16)
             if b == 0:
                 ret_v[q, rs, :] = total
                 continue
@@ -289,57 +320,52 @@
                 where = block(b - 1, r)
                 remote(
                     xs_v.at[q, where, :], ret_v.at[q, where, :],
-                    sem("xs", 0), sem("xr", q), {"ep": flip(me, r)},
+                    sem("xs", 0), sem("xr", q, b - 1), {"ep": flip(me, r)},
                 ).start()
 
     def slab_rows(s):
-        return slice(cap + s * slab, cap + (s + 1) * slab)
-
-    def pass_shared(s):
-        for i in swapped:
-            for r in reversed(range(1, ep)):
-                at = area(i, block(s, r), odd)
-                arrived(at, "dr", i, s, r)
-                remote(at, at, sem("hs", i), sem("hr", i, s), {"tp": beside}).start()
-            relay(i, s, odd)
-
-    def pass_rest(s):
-        whole = pl.ds(cap + s * slab, slab)
-        for i in range(len(pieces)):
-            if i in swapped:
-                arrived(area(i, whole, 1 - odd), "hr", i, s)
-                relay(i, s, 1 - odd)
-        for i in range(len(pieces)):
-            if i not in swapped:
-                arrived(area(i, whole, odd), "dr", i, s)
-                relay(i, s, odd)
+        return slice(bases[s], bases[s] + slabs[s])
 
     def landed(s):
         def ready(a):
-            arrived(all_v.at[a, other, pl.ds(cap + s * slab, slab), :], "yr", a, s)
+            arrived(all_v.at[a, other, whole(s), :], "yr", s, a)
         return ready
+
+    def is_shared(s):
+        return [i for i, piece in enumerate(plan[s]) if piece[3]]
 
     home_rows = slice(0, cap)
     remote_blocks = list(range(1, ep))
-    pass_shared(0)
     for cp in loads[4:]:
         cp.wait()
     if not aligned:
         wcat_ref[...] = jnp.concatenate([wg_ref[...], wl_ref[...]], axis=1)
     forward(0, cap, [0], 0, lambda a: None)
     give(0, home_rows)
-    pass_rest(0)
+    lag = 2
+    turns = []
+    for i in range(len(plan[0])):
+        land(0, i)
+        if plan[0][i][3]:
+            turns.append(i)
+        while len(turns) > lag or (turns and not plan[0][i][3]):
+            turn(0, turns.pop(0))
+    take(0, home_rows)
+    for i in is_shared(1):
+        land(1, i)
     arrived(grow_v.at[pl.ds(1, ep - 1)], "gr", 0)
-    for s in range(SLABS):
-        forward(cap + s * slab, span, remote_blocks, s * span, landed(s))
-        give(1 + s, slab_rows(s))
-        if s == 0:
-            take(0, home_rows)
-        if s + 1 < SLABS:
-            pass_shared(s + 1)
-        take(1 + s, slab_rows(s))
-        if s + 1 < SLABS:
-            pass_rest(s + 1)
+    forward(bases[0], cuts[0], remote_blocks, ranks[0], landed(0))
+    give(1, slab_rows(0))
+    rest = [i for i in range(len(plan[1])) if not plan[1][i][3]]
+    for i in rest[:-1]:
+        land(1, i)
+    for i in is_shared(1):
+        turn(1, i)
+    take(1, slab_rows(0))
+    land(1, rest[-1])
+    forward(bases[1], cuts[1], remote_blocks, ranks[1], landed(1))
+    give(2, slab_rows(1))
+    take(2, slab_rows(1))
 
     for q in range(1, tp):
         remote(
@@ -347,6 +373,27 @@
             {"tp": lax.rem(tpi + q, tp)},
         ).start()
 
+    marks = [0, ranks[1], rows]
+
+    def combine(s):
+        kept = None
+        lines = slice(marks[s], marks[s + 1])
+        at = pl.ds(marks[s], marks[s + 1] - marks[s])
+        deep = bases[s] + slabs[s]
+        for q in order:
+            arrived(ret_v.at[q, whole(s), :], "xr", q, s)
+            part = dot_nn(pt_v[lines, 0:deep], ret_v[q, 0:deep, :])
+            if q == 0:
+                kept = part
+                continue
+            zs_v[q, lines, :] = part.astype(bf16)
+            remote(
+                zs_v.at[q, at, :], zr_v.at[q, at, :], sem("zs", 0), sem("zr", s),
+                {"tp": flip(chip, q) * CORES + core},
+            ).start()
+        return kept
+
+    kept = [combine(0)]
     tr_v[0:2 * units, :] = bf_v[...].astype(f32).T.astype(bf16)
     tr_v[2 * units:3 * units, :] = hg_v[...].astype(f32).T.astype(bf16)
     step = min(512, half)
@@ -358,10 +405,11 @@
                 wn = w[n * units:(n + 1) * units, :]
                 ns_v[n:n + 1, cols] = jnp.sum(wn * wn, axis=0, keepdims=True)
                 w_v[cols, :] = wn.T
-    nr_v[tpi] = ns_v[...]
+    nr_v[tpi] = ns_v[...].astype(bf16)
     for q in range(1, tp):
         remote(
-            ns_v, nr_v.at[tpi], sem("ns", 0), sem("nr", 0), {"tp": lax.rem(tpi + q, tp)}
+            nr_v.at[tpi], nr_v.at[tpi], sem("ns", 0), sem("nr", 0),
+            {"tp": lax.rem(tpi + q, tp)},
         ).start()
 
     arrived(gp_v.at[pl.ds(1, tp - 1)], "ar", 0)
@@ -374,7 +422,6 @@
         remote(
             gsum_v.at[r], gback_v.at[r], sem("bs", 0), sem("br", 0), {"ep": flip(me, r)}
         ).start()
-
     norm = jnp.zeros((units, 1), f32)
     for h in range(CORES):
         for c0 in range(0, half, step):
@@ -387,19 +434,7 @@
     )
     dn_ref[...] = jnp.sum(jnp.where(diag, norm, 0.0), axis=0, keepdims=True)
 
-    acc = None
-    for q in order:
-        arrived(ret_v.at[q, pl.ds(cap, far), :], "xr", q)
-        part = dot_nn(pt_v[...], ret_v[q])
-        if q == 0:
-            acc = part
-        else:
-            zs_v[q] = part.astype(bf16)
-            remote(
-                zs_v.at[q], zr_v.at[q], sem("zs", 0), sem("zr", 0),
-                {"tp": flip(chip, q) * CORES + core},
-            ).start()
-
+    kept.append(combine(1))
     arrived(gback_v.at[pl.ds(1, ep - 1)], "br", 0)
     res = [jnp.zeros((1, rows), f32), jnp.zeros((1, rows), f32)]
     for r in range(ep):
@@ -411,26 +446,31 @@
     dgate_ref[1:2, :] = res[1]
 
     arrived(nr_v.at[pl.ds(1, tp - 1)], "nr", 0)
-    norms = nr_v[0]
+    norms = nr_v[0].astype(f32)
     for j in range(1, tp):
-        norms = norms + nr_v[j]
+        norms = norms + nr_v[j].astype(f32)
     gn_ref[...] = norms[0:1, :]
     ln_ref[...] = norms[1:2, :]
 
-    if nz > 1:
-        arrived(zr_v.at[pl.ds(1, nz - 1)], "zr", 0)
-    for q in range(1, nz):
-        acc = acc + zr_v[q].astype(f32)
-    dtok_ref[...] = acc.astype(bf16)
+    for s in range(len(cuts)):
+        lines = slice(marks[s], marks[s + 1])
+        at = pl.ds(marks[s], marks[s + 1] - marks[s])
+        acc = kept[s]
+        if nz > 1:
+            arrived(zr_v.at[pl.ds(1, nz - 1), at, :], "zr", s)
+        for q in range(1, nz):
+            acc = acc + zr_v[q, lines, :].astype(f32)
+        dtok_ref[lines, :] = acc.astype(bf16)
 
     remote_rows = pl.ds(cap, far)
-    for i in range(len(pieces)):
-        a, cols = window(i, odd)
-        sent(snd_v.at[a, :, cols], "ds", i)
-        if i in swapped:
-            sent(area(i, remote_rows, odd), "hs", i)
+    for s in range(len(cuts)):
+        for i, (a, off, w, shared) in enumerate(plan[s]):
+            cols = window(s, i, odd)[1]
+            sent(snd_v.at[a, pl.ds(bases[s] - cap, slabs[s]), cols], "ds", 0)
+            if shared:
+                sent(area(s, i, whole(s), odd), "hs", 0)
     for a in range(2):
-        sent(all_v.at[a, core, remote_rows, :], "ys", a)
+        sent(all_v.at[a, core, remote_rows, :], "ys", 0)
     sent(gsnd_v.at[pl.ds(1, ep - 1)], "gs", 0)
     sent(ps_v, "ps", 0)
     sent(xs_v.at[:, remote_rows, :], "xs", 0)
@@ -459,7 +499,7 @@
     width = tokens.shape[1]
     units = w_glu.shape[2]
     cap = 3 * rows * top // (2 * ep)
-    cap = -(-cap // (16 * SLABS)) * (16 * SLABS)
+    cap = -(-cap // 32) * 32
     slots = ep * cap
     half = width // CORES
     own = width // tp
@@ -504,7 +544,6 @@
             V((3 * units, slots), bf16),
             V((nz, slots, own), bf16),
             V((nz, slots, own), bf16),
-            V((nz, slots, own), f32),
             V((nz, slots, own), bf16),
             V((nz, slots, own), bf16),
             V((nz, rows, own), bf16),
@@ -513,7 +552,7 @@
             V((ep, 8, LANES), f32),
             V((ep, 8, LANES), f32),
             V((2, width), f32),
-            V((tp, 2, width), f32),
+            V((tp, 2, width), bf16),
             dma((len(semaphores(ep, nz, piece_list(half))),)),
         ],
         compiler_params=pltpu.CompilerParams(

time: 46.1 us -> 40 us (0.87)
  Pallas kernels: 45.3 us -> 39.2 us
    pallas_call x1, Pallas kernels: 43.6 us -> 37.4 us  [shards(): pl.pallas_call(functools.partial(kernel, ep, tp, cap), out_shape=out_shap...]
where the time goes in v2:
time: 40 us; the launch traced here: 39.8 us
  Pallas kernels  39.2 us (98%)
  between operations  0.64 us (2%)
    pallas_call x1, Pallas kernels, shards(): pl.pallas_call(functools.partial(kernel, ep, tp, cap), out_shape=out_shap...  37.4 us
    pallas_call x1, Pallas kernels, shards(): pl.pallas_call(write_out, out_shape=out_shape, in_specs=[vm] * len(out_sh...  1.77 us

profile of v2, /device:TPU:0, one launch (start us, length us, event | category | flops | bytes accessed | tf_op | source)
XLA Modules:
  0.0 39.8 jit_solution(4193543928028914345)
XLA Ops:
  0.6 37.4 %shard_map.134 = (bf16[128,256]{1,0:T(8,128)(2,1)S(1)}, f32[2,128]{1,0:T(2,128)S(1)}, f32[2048,128]{1,0:T(8,128)S(1)}, f32[2048,128]{1,0:T(8,128)S(1)}, f32[128,...) custom-call(bf16[128,2048]{1,0:T(8,128)(2,1)} %tok_hbm.1, ...), custom_call_target="tpu_custom_call" | custom-call | tf_op jit(solution)/shard_map/pallas_call | solution.py:522
  38.1 1.8 %shard_map.135 = (bf16[128,256]{1,0:T(8,128)(2,1)}, f32[2,128]{1,0:T(2,128)}, f32[2048,128]{1,0:T(8,128)}, f32[2048,128]{1,0:T(8,128)}, f32[128,2048]{1,0:T(8,12...) custom-call(bf16[128,256]{1,0:T(8,128)(2,1)S(1)} %get-tuple-element.24.refs_0_, ...), custom_call_target="tpu_custom_call" | custom-call | tf_op jit(solution)/shard_map/pallas_call | solution.py:564

commit v3 on v2

--- a/solution.py
+++ b/solution.py
@@ -70,7 +70,7 @@
 def semaphores(ep, nz, plan):
     keys = [("load", i) for i in range(7)]
     keys += [(k, 0) for k in ("gs", "ps", "xs", "zs", "as", "bs", "ns", "ds", "hs", "ys")]
-    keys += [(k, 0) for k in ("gr", "ar", "br", "nr")]
+    keys += [(k, 0) for k in ("gr", "ar", "br", "nr", "ur", "us")]
     for s, pieces in enumerate(plan):
         for i, piece in enumerate(pieces):
             keys.append(("dr", s, i))
@@ -90,8 +90,8 @@
     dtok_ref, dgate_ref, gw_v, lw_v, dw_v, gn_ref, ln_ref, dn_ref,
     tok_ref, routes_ref, gates_ref, cot_ref, wg_ref, wl_ref, wcat_ref, wd_ref,
     pt_v, pk_v, snd_v, all_v, gsnd_v, grow_v, bf_v, hg_v, tr_v,
-    ps_v, pr_v, xs_v, ret_v, zs_v, zr_v,
-    gp_v, gsum_v, gback_v, ns_v, nr_v, sem_v,
+    ps_v, pr_v, mine_v, xs_v, ret_v, zs_v, zr_v,
+    gp_v, gsum_v, gback_v, ns_v, np_v, nr_v, sem_v,
 ):
     me = lax.axis_index("ep")
     tpi = lax.axis_index("tp")
@@ -153,7 +153,7 @@
     loads[0].wait()
     loads[1].wait()
     rel = jnp.bitwise_xor(routes_ref[...], me)
-    erows = gp_v.shape[1]
+    erows = max(8, ep)
     sub = lax.broadcasted_iota(jnp.int32, (erows, rows), 0)
     first, second = sub == rel[0:1, :], sub == rel[1:2, :]
     mask = jnp.where(first, 1.0, 0.0) + jnp.where(second, 1.0, 0.0)
@@ -301,17 +301,19 @@
         at = pl.ds(rs.start, rs.stop - rs.start)
         for q in order:
             ps_v[q, rs, :] = input_cols(q, other, rs).astype(bf16)
+        for q in order:
             remote(
                 ps_v.at[q, at, :], pr_v.at[q, at, :], sem("ps", 0), sem("pr", q, b),
                 {"tp": partner},
             ).start()
+        for q in order:
+            mine_v[q, rs, :] = input_cols(q, core, rs)
 
     def take(b, rs):
         at = pl.ds(rs.start, rs.stop - rs.start)
         for q in order:
-            mine = input_cols(q, core, rs)
             arrived(pr_v.at[q, at, :], "pr", q, b)
-            total = (mine + pr_v[q, rs, :].astype(f32)).astype(bf16)
+            total = (mine_v[q, rs, :] + pr_v[q, rs, :].astype(f32)).astype(bf16)
             if b == 0:
                 ret_v[q, rs, :] = total
                 continue
@@ -328,11 +330,34 @@
 
     def landed(s):
         def ready(a):
+            if a == 0 and s == 0:
+                for i in is_shared(1):
+                    land(1, i)
             arrived(all_v.at[a, other, whole(s), :], "yr", s, a)
         return ready
 
     def is_shared(s):
         return [i for i, piece in enumerate(plan[s]) if piece[3]]
+
+    marks = [0, ranks[1], rows]
+
+    def combine(s, which):
+        kept = None
+        lines = slice(marks[s], marks[s + 1])
+        at = pl.ds(marks[s], marks[s + 1] - marks[s])
+        deep = bases[s] + slabs[s]
+        for q in which:
+            arrived(ret_v.at[q, whole(s), :], "xr", q, s)
+            part = dot_nn(pt_v[lines, 0:deep], ret_v[q, 0:deep, :])
+            if q == 0:
+                kept = part
+                continue
+            zs_v[q, lines, :] = part.astype(bf16)
+            remote(
+                zs_v.at[q, at, :], zr_v.at[q, at, :], sem("zs", 0), sem("zr", s),
+                {"tp": flip(chip, q) * CORES + core},
+            ).start()
+        return kept
 
     home_rows = slice(0, cap)
     remote_blocks = list(range(1, ep))
@@ -346,54 +371,32 @@
     turns = []
     for i in range(len(plan[0])):
         land(0, i)
+        if i == 3:
+            take(0, home_rows)
         if plan[0][i][3]:
             turns.append(i)
         while len(turns) > lag or (turns and not plan[0][i][3]):
             turn(0, turns.pop(0))
-    take(0, home_rows)
-    for i in is_shared(1):
-        land(1, i)
     arrived(grow_v.at[pl.ds(1, ep - 1)], "gr", 0)
     forward(bases[0], cuts[0], remote_blocks, ranks[0], landed(0))
     give(1, slab_rows(0))
     rest = [i for i in range(len(plan[1])) if not plan[1][i][3]]
+    take(1, slab_rows(0))
     for i in rest[:-1]:
         land(1, i)
     for i in is_shared(1):
         turn(1, i)
-    take(1, slab_rows(0))
     land(1, rest[-1])
     forward(bases[1], cuts[1], remote_blocks, ranks[1], landed(1))
     give(2, slab_rows(1))
+    combine(0, order[:1])
     take(2, slab_rows(1))
-
     for q in range(1, tp):
         remote(
             gp_v.at[tpi], gp_v.at[tpi], sem("as", 0), sem("ar", 0),
             {"tp": lax.rem(tpi + q, tp)},
         ).start()
-
-    marks = [0, ranks[1], rows]
-
-    def combine(s):
-        kept = None
-        lines = slice(marks[s], marks[s + 1])
-        at = pl.ds(marks[s], marks[s + 1] - marks[s])
-        deep = bases[s] + slabs[s]
-        for q in order:
-            arrived(ret_v.at[q, whole(s), :], "xr", q, s)
-            part = dot_nn(pt_v[lines, 0:deep], ret_v[q, 0:deep, :])
-            if q == 0:
-                kept = part
-                continue
-            zs_v[q, lines, :] = part.astype(bf16)
-            remote(
-                zs_v.at[q, at, :], zr_v.at[q, at, :], sem("zs", 0), sem("zr", s),
-                {"tp": flip(chip, q) * CORES + core},
-            ).start()
-        return kept
-
-    kept = [combine(0)]
+    kept = [combine(0, order[1:])]
     tr_v[0:2 * units, :] = bf_v[...].astype(f32).T.astype(bf16)
     tr_v[2 * units:3 * units, :] = hg_v[...].astype(f32).T.astype(bf16)
     step = min(512, half)
@@ -405,23 +408,8 @@
                 wn = w[n * units:(n + 1) * units, :]
                 ns_v[n:n + 1, cols] = jnp.sum(wn * wn, axis=0, keepdims=True)
                 w_v[cols, :] = wn.T
-    nr_v[tpi] = ns_v[...].astype(bf16)
-    for q in range(1, tp):
-        remote(
-            nr_v.at[tpi], nr_v.at[tpi], sem("ns", 0), sem("nr", 0),
-            {"tp": lax.rem(tpi + q, tp)},
-        ).start()
-
-    arrived(gp_v.at[pl.ds(1, tp - 1)], "ar", 0)
-    gsum = gp_v[0]
-    for j in range(1, tp):
-        gsum = gsum + gp_v[j]
-    gback_v[0, 0:1, :] = gsum[0:1, :]
-    for r in range(1, ep):
-        gsum_v[r] = jnp.broadcast_to(gsum[r:r + 1, :], (8, LANES))
-        remote(
-            gsum_v.at[r], gback_v.at[r], sem("bs", 0), sem("br", 0), {"ep": flip(me, r)}
-        ).start()
+    remote(ns_v, np_v, sem("us", 0), sem("ur", 0), {"tp": partner}).start()
+
     norm = jnp.zeros((units, 1), f32)
     for h in range(CORES):
         for c0 in range(0, half, step):
@@ -434,7 +422,27 @@
     )
     dn_ref[...] = jnp.sum(jnp.where(diag, norm, 0.0), axis=0, keepdims=True)
 
-    kept.append(combine(1))
+
+    arrived(np_v, "ur", 0)
+    nr_v[chip] = (ns_v[...] + np_v[...]).astype(bf16)
+    mine_cols = pl.ds(pl.multiple_of(core * half, LANES), half)
+    for z in range(1, nz):
+        for c in range(CORES):
+            at = nr_v.at[chip, :, mine_cols]
+            remote(
+                at, at, sem("ns", 0), sem("nr", 0), {"tp": flip(chip, z) * CORES + c}
+            ).start()
+    arrived(gp_v.at[pl.ds(1, tp - 1)], "ar", 0)
+    gsum = gp_v[0]
+    for j in range(1, tp):
+        gsum = gsum + gp_v[j]
+    gback_v[0, 0:1, :] = gsum[0:1, :]
+    for r in range(1, ep):
+        gsum_v[r] = jnp.broadcast_to(gsum[r:r + 1, :], (8, LANES))
+        remote(
+            gsum_v.at[r], gback_v.at[r], sem("bs", 0), sem("br", 0), {"ep": flip(me, r)}
+        ).start()
+    kept.append(combine(1, order))
     arrived(gback_v.at[pl.ds(1, ep - 1)], "br", 0)
     res = [jnp.zeros((1, rows), f32), jnp.zeros((1, rows), f32)]
     for r in range(ep):
@@ -445,9 +453,10 @@
     dgate_ref[0:1, :] = res[0]
     dgate_ref[1:2, :] = res[1]
 
-    arrived(nr_v.at[pl.ds(1, tp - 1)], "nr", 0)
+    if nz > 1:
+        arrived(nr_v.at[pl.ds(1, nz - 1)], "nr", 0)
     norms = nr_v[0].astype(f32)
-    for j in range(1, tp):
+    for j in range(1, nz):
         norms = norms + nr_v[j].astype(f32)
     gn_ref[...] = norms[0:1, :]
     ln_ref[...] = norms[1:2, :]
@@ -478,7 +487,9 @@
         sent(zs_v.at[pl.ds(1, nz - 1)], "zs", 0)
     sent(gp_v.at[pl.ds(1, tp - 1)], "as", 0)
     sent(gsum_v.at[pl.ds(1, ep - 1)], "bs", 0)
-    sent(nr_v.at[pl.ds(1, tp - 1)], "ns", 0)
+    sent(ns_v, "us", 0)
+    if nz > 1:
+        sent(nr_v.at[pl.ds(1, nz - 1)], "ns", 0)
 
 
 def write_out(*refs):
@@ -507,7 +518,6 @@
     vm = pl.BlockSpec(memory_space=pltpu.VMEM)
     hbm = pl.BlockSpec(memory_space=pltpu.HBM)
     dma = pltpu.SemaphoreType.DMA
-    erows = max(8, ep)
     V = pltpu.VMEM
     out_shape = (
         jax.ShapeDtypeStruct((rows, own), bf16),
@@ -544,15 +554,17 @@
             V((3 * units, slots), bf16),
             V((nz, slots, own), bf16),
             V((nz, slots, own), bf16),
+            V((nz, slots, own), f32),
             V((nz, slots, own), bf16),
             V((nz, slots, own), bf16),
             V((nz, rows, own), bf16),
             V((nz, rows, own), bf16),
-            V((tp, erows, LANES), f32),
+            V((tp, ep, LANES), f32),
             V((ep, 8, LANES), f32),
             V((ep, 8, LANES), f32),
             V((2, width), f32),
-            V((tp, 2, width), bf16),
+            V((2, width), f32),
+            V((nz, 2, width), bf16),
             dma((len(semaphores(ep, nz, piece_list(half))),)),
         ],
         compiler_params=pltpu.CompilerParams(

time: 40 us -> 38.9 us (0.972)
  Pallas kernels: 39.2 us -> 38.1 us
    pallas_call x1, Pallas kernels: 37.4 us -> 36.3 us  [shards(): pl.pallas_call(functools.partial(kernel, ep, tp, cap), out_shape=out_shap...]
where the time goes in v3:
time: 38.9 us; the launch traced here: 38.7 us
  Pallas kernels  38.1 us (98%)
  between operations  0.64 us (2%)
    pallas_call x1, Pallas kernels, shards(): pl.pallas_call(functools.partial(kernel, ep, tp, cap), out_shape=out_shap...  36.3 us
    pallas_call x1, Pallas kernels, shards(): pl.pallas_call(write_out, out_shape=out_shape, in_specs=[vm] * len(out_sh...  1.77 us

profile of v3, /device:TPU:0, one launch (start us, length us, event | category | flops | bytes accessed | tf_op | source)
XLA Modules:
  0.0 38.7 jit_solution(15193220291230819392)
XLA Ops:
  0.6 36.3 %shard_map.134 = (bf16[128,256]{1,0:T(8,128)(2,1)S(1)}, f32[2,128]{1,0:T(2,128)S(1)}, f32[2048,128]{1,0:T(8,128)S(1)}, f32[2048,128]{1,0:T(8,128)S(1)}, f32[128,...) custom-call(bf16[128,2048]{1,0:T(8,128)(2,1)} %tok_hbm.1, ...), custom_call_target="tpu_custom_call" | custom-call | tf_op jit(solution)/shard_map/pallas_call | solution.py:532
  36.9 1.8 %shard_map.135 = (bf16[128,256]{1,0:T(8,128)(2,1)}, f32[2,128]{1,0:T(2,128)}, f32[2048,128]{1,0:T(8,128)}, f32[2048,128]{1,0:T(8,128)}, f32[128,2048]{1,0:T(8,12...) custom-call(bf16[128,256]{1,0:T(8,128)(2,1)S(1)} %get-tuple-element.24.refs_0_, ...), custom_call_target="tpu_custom_call" | custom-call | tf_op jit(solution)/shard_map/pallas_call | solution.py:576

commit v4 on v3

--- a/solution.py
+++ b/solution.py
@@ -13,7 +13,9 @@
 LANES = 128
 CORES = 2
 SHARE = 3
-FLIGHT = 6
+FLIGHT = 8
+LATE = 12
+FIRST = 4
 f32 = jnp.float32
 bf16 = jnp.bfloat16
 
@@ -49,11 +51,12 @@
 
 
 def slab_cuts(cap):
-    first = min(-(-2 * cap // 48) * 16, cap - 16)
-    return (first, cap - first)
-
-
-def piece_list(half):
+    tiles = cap // 16
+    first = min(-(-tiles * FIRST // 6), tiles - 1)
+    return (16 * first, 16 * (tiles - first))
+
+
+def piece_list(half, count):
     unit = half // 8
     early = tuple((1, 2 * k * unit, unit, True) for k in range(4)) + (
         (0, 0, unit, True),
@@ -64,13 +67,13 @@
         (0, 0, half // 2, False),
         (0, half // 2, half // 2, False),
     )
-    return (early, late)
+    return (early,) + (late,) * (count - 1)
 
 
 def semaphores(ep, nz, plan):
     keys = [("load", i) for i in range(7)]
-    keys += [(k, 0) for k in ("gs", "ps", "xs", "zs", "as", "bs", "ns", "ds", "hs", "ys")]
-    keys += [(k, 0) for k in ("gr", "ar", "br", "nr", "ur", "us")]
+    keys.append(("out", 0))
+    keys += [(k, 0) for k in ("gr", "ar", "br", "nr", "ur")]
     for s, pieces in enumerate(plan):
         for i, piece in enumerate(pieces):
             keys.append(("dr", s, i))
@@ -112,7 +115,7 @@
     bases = [cap + sum(slabs[:s]) for s in range(len(cuts))]
     ranks = [sum(cuts[:s]) for s in range(len(cuts))]
     far = sum(slabs)
-    plan = piece_list(half)
+    plan = piece_list(half, len(cuts))
     table = semaphores(ep, nz, plan)
 
     def sem(*key):
@@ -193,7 +196,7 @@
 
     def relay(s, i, whose):
         at = area(s, i, whole(s), whose)
-        remote(at, at, sem("ys", 0), sem("yr", s, plan[s][i][0]), {"tp": partner}).start()
+        remote(at, at, sem("out", 0), sem("yr", s, plan[s][i][0]), {"tp": partner}).start()
 
     steps = [(s, i) for s in range(len(cuts)) for i in range(len(plan[s]))]
     state = {"next": 0, "load": 0, "waited": False}
@@ -215,20 +218,24 @@
         for r in reversed(range(1, ep)):
             remote(
                 snd_v.at[a, pl.ds(at + (r - 1) * cuts[s], cuts[s]), cols],
-                area(s, i, block(s, r), odd), sem("ds", 0), sem("dr", s, i), {"ep": flip(me, r)},
+                area(s, i, block(s, r), odd), sem("out", 0), sem("dr", s, i), {"ep": flip(me, r)},
             ).start()
         state["next"] += 1
         state["load"] += cost(s, i)
 
+    def limit():
+        units = FLIGHT if steps[state["next"]][0] == 0 else LATE
+        return units * cuts[0] * half // 8
+
     def fill():
-        while state["next"] < len(steps) and state["load"] < FLIGHT * cuts[0] * half // 8:
+        while state["next"] < len(steps) and state["load"] < limit():
             dispatch()
 
     def land(s, i):
         at = area(s, i, whole(s), odd)
         arrived(at, "dr", s, i)
         if plan[s][i][3]:
-            remote(at, at, sem("hs", 0), sem("hr", s, i), {"tp": beside}).start()
+            remote(at, at, sem("out", 0), sem("hr", s, i), {"tp": beside}).start()
         relay(s, i, odd)
         state["load"] -= cost(s, i)
         fill()
@@ -248,7 +255,7 @@
         else:
             gsnd_v[r] = jnp.broadcast_to(row, (8, LANES))
             remote(
-                gsnd_v.at[r], grow_v.at[r], sem("gs", 0), sem("gr", 0), {"ep": flip(me, r)}
+                gsnd_v.at[r], grow_v.at[r], sem("out", 0), sem("gr", 0), {"ep": flip(me, r)}
             ).start()
     home = hits[0][:cap, :].astype(bf16)
     for a, ref in ((0, tok_ref), (1, cot_ref)):
@@ -303,7 +310,7 @@
             ps_v[q, rs, :] = input_cols(q, other, rs).astype(bf16)
         for q in order:
             remote(
-                ps_v.at[q, at, :], pr_v.at[q, at, :], sem("ps", 0), sem("pr", q, b),
+                ps_v.at[q, at, :], pr_v.at[q, at, :], sem("out", 0), sem("pr", q, b),
                 {"tp": partner},
             ).start()
         for q in order:
@@ -322,7 +329,7 @@
                 where = block(b - 1, r)
                 remote(
                     xs_v.at[q, where, :], ret_v.at[q, where, :],
-                    sem("xs", 0), sem("xr", q, b - 1), {"ep": flip(me, r)},
+                    sem("out", 0), sem("xr", q, b - 1), {"ep": flip(me, r)},
                 ).start()
 
     def slab_rows(s):
@@ -330,16 +337,16 @@
 
     def landed(s):
         def ready(a):
-            if a == 0 and s == 0:
-                for i in is_shared(1):
-                    land(1, i)
+            if a == 0 and s + 1 < len(cuts):
+                for i in is_shared(s + 1):
+                    land(s + 1, i)
             arrived(all_v.at[a, other, whole(s), :], "yr", s, a)
         return ready
 
     def is_shared(s):
         return [i for i, piece in enumerate(plan[s]) if piece[3]]
 
-    marks = [0, ranks[1], rows]
+    marks = ranks + [rows]
 
     def combine(s, which):
         kept = None
@@ -354,7 +361,7 @@
                 continue
             zs_v[q, lines, :] = part.astype(bf16)
             remote(
-                zs_v.at[q, at, :], zr_v.at[q, at, :], sem("zs", 0), sem("zr", s),
+                zs_v.at[q, at, :], zr_v.at[q, at, :], sem("out", 0), sem("zr", s),
                 {"tp": flip(chip, q) * CORES + core},
             ).start()
         return kept
@@ -378,25 +385,25 @@
         while len(turns) > lag or (turns and not plan[0][i][3]):
             turn(0, turns.pop(0))
     arrived(grow_v.at[pl.ds(1, ep - 1)], "gr", 0)
-    forward(bases[0], cuts[0], remote_blocks, ranks[0], landed(0))
-    give(1, slab_rows(0))
-    rest = [i for i in range(len(plan[1])) if not plan[1][i][3]]
-    take(1, slab_rows(0))
-    for i in rest[:-1]:
-        land(1, i)
-    for i in is_shared(1):
-        turn(1, i)
-    land(1, rest[-1])
-    forward(bases[1], cuts[1], remote_blocks, ranks[1], landed(1))
-    give(2, slab_rows(1))
-    combine(0, order[:1])
-    take(2, slab_rows(1))
+    last = len(cuts) - 1
+    for s in range(last):
+        forward(bases[s], cuts[s], remote_blocks, ranks[s], landed(s))
+        give(1 + s, slab_rows(s))
+        take(1 + s, slab_rows(s))
+        rest = [i for i in range(len(plan[s + 1])) if not plan[s + 1][i][3]]
+        for i in rest[:-1]:
+            land(s + 1, i)
+        for i in is_shared(s + 1):
+            turn(s + 1, i)
+        land(s + 1, rest[-1])
+    forward(bases[last], cuts[last], remote_blocks, ranks[last], landed(last))
     for q in range(1, tp):
         remote(
-            gp_v.at[tpi], gp_v.at[tpi], sem("as", 0), sem("ar", 0),
+            gp_v.at[tpi], gp_v.at[tpi], sem("out", 0), sem("ar", 0),
             {"tp": lax.rem(tpi + q, tp)},
         ).start()
-    kept = [combine(0, order[1:])]
+    give(1 + last, slab_rows(last))
+    combine(0, order[:1])
     tr_v[0:2 * units, :] = bf_v[...].astype(f32).T.astype(bf16)
     tr_v[2 * units:3 * units, :] = hg_v[...].astype(f32).T.astype(bf16)
     step = min(512, half)
@@ -408,7 +415,9 @@
                 wn = w[n * units:(n + 1) * units, :]
                 ns_v[n:n + 1, cols] = jnp.sum(wn * wn, axis=0, keepdims=True)
                 w_v[cols, :] = wn.T
-    remote(ns_v, np_v, sem("us", 0), sem("ur", 0), {"tp": partner}).start()
+    remote(ns_v, np_v, sem("out", 0), sem("ur", 0), {"tp": partner}).start()
+    take(1 + last, slab_rows(last))
+    kept = [combine(0, order[1:])]
 
     norm = jnp.zeros((units, 1), f32)
     for h in range(CORES):
@@ -422,7 +431,6 @@
     )
     dn_ref[...] = jnp.sum(jnp.where(diag, norm, 0.0), axis=0, keepdims=True)
 
-
     arrived(np_v, "ur", 0)
     nr_v[chip] = (ns_v[...] + np_v[...]).astype(bf16)
     mine_cols = pl.ds(pl.multiple_of(core * half, LANES), half)
@@ -430,7 +438,7 @@
         for c in range(CORES):
             at = nr_v.at[chip, :, mine_cols]
             remote(
-                at, at, sem("ns", 0), sem("nr", 0), {"tp": flip(chip, z) * CORES + c}
+                at, at, sem("out", 0), sem("nr", 0), {"tp": flip(chip, z) * CORES + c}
             ).start()
     arrived(gp_v.at[pl.ds(1, tp - 1)], "ar", 0)
     gsum = gp_v[0]
@@ -440,9 +448,10 @@
     for r in range(1, ep):
         gsum_v[r] = jnp.broadcast_to(gsum[r:r + 1, :], (8, LANES))
         remote(
-            gsum_v.at[r], gback_v.at[r], sem("bs", 0), sem("br", 0), {"ep": flip(me, r)}
+            gsum_v.at[r], gback_v.at[r], sem("out", 0), sem("br", 0), {"ep": flip(me, r)}
         ).start()
-    kept.append(combine(1, order))
+    for s in range(1, len(cuts)):
+        kept.append(combine(s, order))
     arrived(gback_v.at[pl.ds(1, ep - 1)], "br", 0)
     res = [jnp.zeros((1, rows), f32), jnp.zeros((1, rows), f32)]
     for r in range(ep):
@@ -475,21 +484,21 @@
     for s in range(len(cuts)):
         for i, (a, off, w, shared) in enumerate(plan[s]):
             cols = window(s, i, odd)[1]
-            sent(snd_v.at[a, pl.ds(bases[s] - cap, slabs[s]), cols], "ds", 0)
+            sent(snd_v.at[a, pl.ds(bases[s] - cap, slabs[s]), cols], "out", 0)
             if shared:
-                sent(area(s, i, whole(s), odd), "hs", 0)
+                sent(area(s, i, whole(s), odd), "out", 0)
     for a in range(2):
-        sent(all_v.at[a, core, remote_rows, :], "ys", 0)
-    sent(gsnd_v.at[pl.ds(1, ep - 1)], "gs", 0)
-    sent(ps_v, "ps", 0)
-    sent(xs_v.at[:, remote_rows, :], "xs", 0)
+        sent(all_v.at[a, core, remote_rows, :], "out", 0)
+    sent(gsnd_v.at[pl.ds(1, ep - 1)], "out", 0)
+    sent(ps_v, "out", 0)
+    sent(xs_v.at[:, remote_rows, :], "out", 0)
     if nz > 1:
-        sent(zs_v.at[pl.ds(1, nz - 1)], "zs", 0)
-    sent(gp_v.at[pl.ds(1, tp - 1)], "as", 0)
-    sent(gsum_v.at[pl.ds(1, ep - 1)], "bs", 0)
-    sent(ns_v, "us", 0)
+        sent(zs_v.at[pl.ds(1, nz - 1)], "out", 0)
+    sent(gp_v.at[pl.ds(1, tp - 1)], "out", 0)
+    sent(gsum_v.at[pl.ds(1, ep - 1)], "out", 0)
+    sent(ns_v, "out", 0)
     if nz > 1:
-        sent(nr_v.at[pl.ds(1, nz - 1)], "ns", 0)
+        sent(nr_v.at[pl.ds(1, nz - 1)], "out", 0)
 
 
 def write_out(*refs):
@@ -565,7 +574,7 @@
             V((2, width), f32),
             V((2, width), f32),
             V((nz, 2, width), bf16),
-            dma((len(semaphores(ep, nz, piece_list(half))),)),
+            dma((len(semaphores(ep, nz, piece_list(half, len(slab_cuts(cap))))),)),
         ],
         compiler_params=pltpu.CompilerParams(
             collective_id=0, has_side_effects=True, vmem_limit_bytes=28 * 1024 * 1024

time: 38.9 us -> 36.2 us (0.931)
  Pallas kernels: 38.1 us -> 35.4 us
    pallas_call x1, Pallas kernels: 36.3 us -> 33.6 us  [shards(): pl.pallas_call(functools.partial(kernel, ep, tp, cap), out_shape=out_shap...]
where the time goes in v4:
time: 36.2 us; the launch traced here: 36.1 us
  Pallas kernels  35.4 us (98%)
  between operations  0.64 us (2%)
    pallas_call x1, Pallas kernels, shards(): pl.pallas_call(functools.partial(kernel, ep, tp, cap), out_shape=out_shap...  33.6 us
    pallas_call x1, Pallas kernels, shards(): pl.pallas_call(write_out, out_shape=out_shape, in_specs=[vm] * len(out_sh...  1.77 us

profile of v4, /device:TPU:0, one launch (start us, length us, event | category | flops | bytes accessed | tf_op | source)
XLA Modules:
  0.0 36.1 jit_solution(7541517044153664769)
XLA Ops:
  0.6 33.6 %shard_map.134 = (bf16[128,256]{1,0:T(8,128)(2,1)S(1)}, f32[2,128]{1,0:T(2,128)S(1)}, f32[2048,128]{1,0:T(8,128)S(1)}, f32[2048,128]{1,0:T(8,128)S(1)}, f32[128,...) custom-call(bf16[128,2048]{1,0:T(8,128)(2,1)} %tok_hbm.1, ...), custom_call_target="tpu_custom_call" | custom-call | tf_op jit(solution)/shard_map/pallas_call | solution.py:541
  34.3 1.8 %shard_map.135 = (bf16[128,256]{1,0:T(8,128)(2,1)}, f32[2,128]{1,0:T(2,128)}, f32[2048,128]{1,0:T(8,128)}, f32[2048,128]{1,0:T(8,128)}, f32[128,2048]{1,0:T(8,12...) custom-call(bf16[128,256]{1,0:T(8,128)(2,1)S(1)} %get-tuple-element.24.refs_0_, ...), custom_call_target="tpu_custom_call" | custom-call | tf_op jit(solution)/shard_map/pallas_call | solution.py:585

commit v5 on v4

--- a/solution.py
+++ b/solution.py
@@ -60,7 +60,9 @@
     unit = half // 8
     early = tuple((1, 2 * k * unit, unit, True) for k in range(4)) + (
         (0, 0, unit, True),
-    ) + tuple((0, (2 + 2 * k) * unit, 2 * unit, False) for k in range(3))
+    ) + tuple((0, (2 + 2 * k) * unit, 2 * unit, False) for k in range(2)) + (
+        (0, 6 * unit, unit, False), (0, 7 * unit, unit, False),
+    )
     late = (
         (1, 0, SHARE * unit, True),
         (1, 2 * SHARE * unit, half - 2 * SHARE * unit, False),
@@ -73,7 +75,7 @@
 def semaphores(ep, nz, plan):
     keys = [("load", i) for i in range(7)]
     keys.append(("out", 0))
-    keys += [(k, 0) for k in ("gr", "ar", "br", "nr", "ur")]
+    keys += [(k, 0) for k in ("gr", "ar", "br", "nr", "ur", "dx", "ye")]
     for s, pieces in enumerate(plan):
         for i, piece in enumerate(pieces):
             keys.append(("dr", s, i))
@@ -92,7 +94,7 @@
     tok_hbm, routes_hbm, gates_hbm, cot_hbm, wg_hbm, wl_hbm, wd_hbm,
     dtok_ref, dgate_ref, gw_v, lw_v, dw_v, gn_ref, ln_ref, dn_ref,
     tok_ref, routes_ref, gates_ref, cot_ref, wg_ref, wl_ref, wcat_ref, wd_ref,
-    pt_v, pk_v, snd_v, all_v, gsnd_v, grow_v, bf_v, hg_v, tr_v,
+    pt_v, pk_v, snd_v, extra_v, all_v, gsnd_v, grow_v, bf_v, hg_v, back_v, tr_v,
     ps_v, pr_v, mine_v, xs_v, ret_v, zs_v, zr_v,
     gp_v, gsum_v, gback_v, ns_v, np_v, nr_v, sem_v,
 ):
@@ -204,9 +206,42 @@
     def cost(s, i):
         return cuts[s] * plan[s][i][2]
 
+    lone = len(plan[0]) - 1
+    lone_off, lone_w = plan[0][lone][1:3]
+    lone_cols = pl.ds(lone_off, lone_w)
+
+    def lone_dispatch():
+        @pl.when(core == CORES - 1)
+        def _():
+            for h, buf in ((CORES - 1, snd_v.at[0, pl.ds(0, slabs[0]), lone_cols]), (0, extra_v)):
+                at = h * half + lone_off
+                buf[...] = dot_nn(picks[0], tok_ref[:, at:at + lone_w]).astype(bf16)
+                for r in reversed(range(1, ep)):
+                    key = ("dr", 0, lone) if h else ("dx", 0)
+                    remote(
+                        buf.at[pl.ds((r - 1) * cuts[0], cuts[0]), :],
+                        all_v.at[0, h, block(0, r), lone_cols],
+                        sem("out", 0), sem(*key), {"ep": flip(me, r)},
+                    ).start()
+
+    def lone_land():
+        @pl.when(core == CORES - 1)
+        def _():
+            for h in reversed(range(CORES)):
+                key = ("dr", 0, lone) if h else ("dx", 0)
+                at = all_v.at[0, h, whole(0), lone_cols]
+                arrived(at, *key)
+                to = sem("yr", 0, 0) if h else sem("ye", 0)
+                remote(at, at, sem("out", 0), to, {"tp": partner}).start()
+
     def dispatch():
         s, i = steps[state["next"]]
         a, off, w, shared = plan[s][i]
+        if (s, i) == (0, lone):
+            lone_dispatch()
+            state["next"] += 1
+            state["load"] += cost(s, i)
+            return
         cols = window(s, i, odd)[1]
         begin = core * half + off + (odd * w if shared else 0)
         src_cols = pl.ds(pl.multiple_of(begin, LANES), w)
@@ -232,6 +267,11 @@
             dispatch()
 
     def land(s, i):
+        if (s, i) == (0, lone):
+            lone_land()
+            state["load"] -= cost(s, i)
+            fill()
+            return
         at = area(s, i, whole(s), odd)
         arrived(at, "dr", s, i)
         if plan[s][i][3]:
@@ -267,24 +307,29 @@
 
     gp_v[tpi] = jnp.zeros(gp_v.shape[1:], f32)
 
+    def backward_half(at, count, blocks, ready):
+        rs = slice(at, at + count * len(blocks))
+        ready(1)
+        back = jnp.zeros((rs.stop - rs.start, units), f32)
+        for h in range(CORES):
+            back = back + dot_nt(all_v[1, h, rs, :], wd_ref[:, h * half:(h + 1) * half])
+        back_v[rs, :] = back
+
     def forward(at, count, blocks, shift, ready):
         eye = lax.broadcasted_iota(jnp.int32, (count, LANES), 0) + shift == (
             lax.broadcasted_iota(jnp.int32, (count, LANES), 1)
         )
         rs = slice(at, at + count * len(blocks))
-        n = rs.stop - rs.start
-        ready(1)
-        back = jnp.zeros((n, units), f32)
-        for h in range(CORES):
-            back = back + dot_nt(all_v[1, h, rs, :], wd_ref[:, h * half:(h + 1) * half])
         gate_col = jnp.concatenate([
             jnp.sum(jnp.where(eye, grow_v[r, 0:1, :], 0.0), axis=1, keepdims=True)
             for r in blocks
         ], axis=0)
+        mine_at = pl.ds(pl.multiple_of(core * half, LANES), half)
+        other_at = pl.ds(pl.multiple_of(other * half, LANES), half)
         ready(0)
-        pre = jnp.zeros((n, 2 * units), f32)
-        for h in range(CORES):
-            pre = pre + dot_nn(all_v[0, h, rs, :], wcat_ref[h * half:(h + 1) * half, :])
+        pre = dot_nn(all_v[0, core, rs, :], wcat_ref[mine_at, :])
+        pre = pre + dot_nn(all_v[0, other, rs, :], wcat_ref[other_at, :])
+        back = back_v[rs, :]
         hidden, glu_bf, lin_bf = clamp_backward(
             pre[:, 0:units], pre[:, units:2 * units], back, gate_col
         )
@@ -340,7 +385,18 @@
             if a == 0 and s + 1 < len(cuts):
                 for i in is_shared(s + 1):
                     land(s + 1, i)
-            arrived(all_v.at[a, other, whole(s), :], "yr", s, a)
+            if (s, a) != (0, 0):
+                arrived(all_v.at[a, other, whole(s), :], "yr", s, a)
+                return
+
+            @pl.when(core == 0)
+            def _():
+                arrived(all_v.at[0, CORES - 1, whole(0), :], "yr", 0, 0)
+                arrived(all_v.at[0, 0, whole(0), lone_cols], "ye", 0)
+
+            @pl.when(core == CORES - 1)
+            def _():
+                arrived(all_v.at[0, 0, whole(0), pl.ds(0, lone_off)], "yr", 0, 0)
         return ready
 
     def is_shared(s):
@@ -372,6 +428,7 @@
         cp.wait()
     if not aligned:
         wcat_ref[...] = jnp.concatenate([wg_ref[...], wl_ref[...]], axis=1)
+    backward_half(0, cap, [0], lambda a: None)
     forward(0, cap, [0], 0, lambda a: None)
     give(0, home_rows)
     lag = 2
@@ -382,11 +439,13 @@
             take(0, home_rows)
         if plan[0][i][3]:
             turns.append(i)
-        while len(turns) > lag or (turns and not plan[0][i][3]):
+        if len(turns) > lag or (turns and not plan[0][i][3]):
             turn(0, turns.pop(0))
     arrived(grow_v.at[pl.ds(1, ep - 1)], "gr", 0)
+    assert not turns
     last = len(cuts) - 1
     for s in range(last):
+        backward_half(bases[s], cuts[s], remote_blocks, landed(s))
         forward(bases[s], cuts[s], remote_blocks, ranks[s], landed(s))
         give(1 + s, slab_rows(s))
         take(1 + s, slab_rows(s))
@@ -396,6 +455,7 @@
         for i in is_shared(s + 1):
             turn(s + 1, i)
         land(s + 1, rest[-1])
+    backward_half(bases[last], cuts[last], remote_blocks, landed(last))
     forward(bases[last], cuts[last], remote_blocks, ranks[last], landed(last))
     for q in range(1, tp):
         remote(
@@ -483,12 +543,26 @@
     remote_rows = pl.ds(cap, far)
     for s in range(len(cuts)):
         for i, (a, off, w, shared) in enumerate(plan[s]):
+            if (s, i) == (0, lone):
+                continue
             cols = window(s, i, odd)[1]
             sent(snd_v.at[a, pl.ds(bases[s] - cap, slabs[s]), cols], "out", 0)
             if shared:
                 sent(area(s, i, whole(s), odd), "out", 0)
-    for a in range(2):
-        sent(all_v.at[a, core, remote_rows, :], "out", 0)
+    sent(all_v.at[1, core, remote_rows, :], "out", 0)
+
+    @pl.when(core == CORES - 1)
+    def _():
+        sent(snd_v.at[0, pl.ds(0, slabs[0]), lone_cols], "out", 0)
+        sent(extra_v, "out", 0)
+        sent(all_v.at[0, CORES - 1, remote_rows, :], "out", 0)
+        sent(all_v.at[0, 0, whole(0), lone_cols], "out", 0)
+
+    @pl.when(core == 0)
+    def _():
+        sent(all_v.at[0, 0, whole(0), pl.ds(0, lone_off)], "out", 0)
+        sent(all_v.at[0, 0, whole(1), :], "out", 0)
+
     sent(gsnd_v.at[pl.ds(1, ep - 1)], "out", 0)
     sent(ps_v, "out", 0)
     sent(xs_v.at[:, remote_rows, :], "out", 0)
@@ -555,11 +629,13 @@
             V((rows, slots), bf16),
             V((ep, LANES, rows), bf16),
             V((2, slots - cap, half), bf16),
+            V(((ep - 1) * slab_cuts(cap)[0], half // 8), bf16),
             V((2, CORES, slots, half), bf16),
             V((ep, 8, LANES), f32),
             V((ep, 8, LANES), f32),
             V((slots, 2 * units), bf16),
             V((slots, units), bf16),
+            V((slots, units), f32),
             V((3 * units, slots), bf16),
             V((nz, slots, own), bf16),
             V((nz, slots, own), bf16),

time: 36.2 us -> 36.2 us (level)
  no operation moved by 1% of the time
where the time goes in v5:
time: 36.2 us; the launch traced here: 36 us
  Pallas kernels  35.4 us (98%)
  between operations  0.64 us (2%)
    pallas_call x1, Pallas kernels, shards(): pl.pallas_call(functools.partial(kernel, ep, tp, cap), out_shape=out_shap...  33.6 us
    pallas_call x1, Pallas kernels, shards(): pl.pallas_call(write_out, out_shape=out_shape, in_specs=[vm] * len(out_sh...  1.77 us

profile of v5, /device:TPU:0, one launch (start us, length us, event | category | flops | bytes accessed | tf_op | source)
XLA Modules:
  0.0 36.0 jit_solution(15251383026638843060)
XLA Ops:
  0.6 33.6 %shard_map.134 = (bf16[128,256]{1,0:T(8,128)(2,1)S(1)}, f32[2,128]{1,0:T(2,128)S(1)}, f32[2048,128]{1,0:T(8,128)S(1)}, f32[2048,128]{1,0:T(8,128)S(1)}, f32[128,...) custom-call(bf16[128,2048]{1,0:T(8,128)(2,1)} %tok_hbm.1, ...), custom_call_target="tpu_custom_call" | custom-call | tf_op jit(solution)/shard_map/pallas_call | solution.py:615
  34.3 1.8 %shard_map.135 = (bf16[128,256]{1,0:T(8,128)(2,1)}, f32[2,128]{1,0:T(2,128)}, f32[2048,128]{1,0:T(8,128)}, f32[2048,128]{1,0:T(8,128)}, f32[128,2048]{1,0:T(8,12...) custom-call(bf16[128,256]{1,0:T(8,128)(2,1)S(1)} %get-tuple-element.24.refs_0_, ...), custom_call_target="tpu_custom_call" | custom-call | tf_op jit(solution)/shard_map/pallas_call | solution.py:661

commit v6 on v5

--- a/solution.py
+++ b/solution.py
@@ -15,6 +15,7 @@
 SHARE = 3
 FLIGHT = 8
 LATE = 12
+EARLY = 1
 FIRST = 4
 f32 = jnp.float32
 bf16 = jnp.bfloat16
@@ -442,15 +443,40 @@
         if len(turns) > lag or (turns and not plan[0][i][3]):
             turn(0, turns.pop(0))
     arrived(grow_v.at[pl.ds(1, ep - 1)], "gr", 0)
-    assert not turns
     last = len(cuts) - 1
+    step = min(512, half)
+
+    def turned():
+        tr_v[0:2 * units, :] = bf_v[...].astype(f32).T.astype(bf16)
+        tr_v[2 * units:3 * units, :] = hg_v[...].astype(f32).T.astype(bf16)
+
+    def up_wgrad(h):
+        for c0 in range(0, half, step):
+            cols = slice(h * half + c0, h * half + c0 + step)
+            w = dot_nn(tr_v[0:2 * units, :], all_v[0, h, :, c0:c0 + step])
+            for n, w_v in enumerate((gw_v, lw_v)):
+                wn = w[n * units:(n + 1) * units, :]
+                ns_v[n:n + 1, cols] = jnp.sum(wn * wn, axis=0, keepdims=True)
+                w_v[cols, :] = wn.T
+
+    def down_wgrad(h):
+        norm = jnp.zeros((units, 1), f32)
+        for c0 in range(0, half, step):
+            cols = slice(h * half + c0, h * half + c0 + step)
+            w = dot_nn(tr_v[2 * units:3 * units, :], all_v[1, h, :, c0:c0 + step])
+            norm = norm + jnp.sum(w * w, axis=1, keepdims=True)
+            dw_v[:, cols] = w
+        return norm
+
     for s in range(last):
         backward_half(bases[s], cuts[s], remote_blocks, landed(s))
         forward(bases[s], cuts[s], remote_blocks, ranks[s], landed(s))
         give(1 + s, slab_rows(s))
+        rest = [i for i in range(len(plan[s + 1])) if not plan[s + 1][i][3]]
+        for i in rest[:EARLY]:
+            land(s + 1, i)
         take(1 + s, slab_rows(s))
-        rest = [i for i in range(len(plan[s + 1])) if not plan[s + 1][i][3]]
-        for i in rest[:-1]:
+        for i in rest[EARLY:-1]:
             land(s + 1, i)
         for i in is_shared(s + 1):
             turn(s + 1, i)
@@ -463,34 +489,18 @@
             {"tp": lax.rem(tpi + q, tp)},
         ).start()
     give(1 + last, slab_rows(last))
-    combine(0, order[:1])
-    tr_v[0:2 * units, :] = bf_v[...].astype(f32).T.astype(bf16)
-    tr_v[2 * units:3 * units, :] = hg_v[...].astype(f32).T.astype(bf16)
-    step = min(512, half)
-    for h in range(CORES):
-        for c0 in range(0, half, step):
-            cols = slice(h * half + c0, h * half + c0 + step)
-            w = dot_nn(tr_v[0:2 * units, :], all_v[0, h, :, c0:c0 + step])
-            for n, w_v in enumerate((gw_v, lw_v)):
-                wn = w[n * units:(n + 1) * units, :]
-                ns_v[n:n + 1, cols] = jnp.sum(wn * wn, axis=0, keepdims=True)
-                w_v[cols, :] = wn.T
+    turned()
+    up_wgrad(0)
+    take(1 + last, slab_rows(last))
+    combine(0, order[0:1])
+    up_wgrad(1)
     remote(ns_v, np_v, sem("out", 0), sem("ur", 0), {"tp": partner}).start()
-    take(1 + last, slab_rows(last))
     kept = [combine(0, order[1:])]
-
-    norm = jnp.zeros((units, 1), f32)
-    for h in range(CORES):
-        for c0 in range(0, half, step):
-            cols = slice(h * half + c0, h * half + c0 + step)
-            w = dot_nn(tr_v[2 * units:3 * units, :], all_v[1, h, :, c0:c0 + step])
-            norm = norm + jnp.sum(w * w, axis=1, keepdims=True)
-            dw_v[:, cols] = w
     diag = lax.broadcasted_iota(jnp.int32, (units, units), 0) == (
         lax.broadcasted_iota(jnp.int32, (units, units), 1)
     )
+    norm = down_wgrad(0) + down_wgrad(1)
     dn_ref[...] = jnp.sum(jnp.where(diag, norm, 0.0), axis=0, keepdims=True)
-
     arrived(np_v, "ur", 0)
     nr_v[chip] = (ns_v[...] + np_v[...]).astype(bf16)
     mine_cols = pl.ds(pl.multiple_of(core * half, LANES), half)

time: 36.2 us -> 36.1 us (level)
  no operation moved by 1% of the time
where the time goes in v6:
time: 36.1 us; the launch traced here: 36 us
  Pallas kernels  35.3 us (98%)
  between operations  0.64 us (2%)
    pallas_call x1, Pallas kernels, shards(): pl.pallas_call(functools.partial(kernel, ep, tp, cap), out_shape=out_shap...  33.6 us
    pallas_call x1, Pallas kernels, shards(): pl.pallas_call(write_out, out_shape=out_shape, in_specs=[vm] * len(out_sh...  1.77 us

profile of v6, /device:TPU:0, one launch (start us, length us, event | category | flops | bytes accessed | tf_op | source)
XLA Modules:
  0.0 36.0 jit_solution(5232927663796719806)
XLA Ops:
  0.6 33.6 %shard_map.134 = (bf16[128,256]{1,0:T(8,128)(2,1)S(1)}, f32[2,128]{1,0:T(2,128)S(1)}, f32[2048,128]{1,0:T(8,128)S(1)}, f32[2048,128]{1,0:T(8,128)S(1)}, f32[128,...) custom-call(bf16[128,2048]{1,0:T(8,128)(2,1)} %tok_hbm.1, ...), custom_call_target="tpu_custom_call" | custom-call | tf_op jit(solution)/shard_map/pallas_call | solution.py:625
  34.2 1.8 %shard_map.135 = (bf16[128,256]{1,0:T(8,128)(2,1)}, f32[2,128]{1,0:T(2,128)}, f32[2048,128]{1,0:T(8,128)}, f32[2048,128]{1,0:T(8,128)}, f32[128,2048]{1,0:T(8,12...) custom-call(bf16[128,256]{1,0:T(8,128)(2,1)S(1)} %get-tuple-element.24.refs_0_, ...), custom_call_target="tpu_custom_call" | custom-call | tf_op jit(solution)/shard_map/pallas_call | solution.py:671
